TPU v7x, 128 devices: a whole 4x4x4 slice. The times are simulated.
128 devices in a mesh: tp: 16 (over z, y), dp: 8 (over x, core).
Axes of the slice: x: 4, y: 4, z: 4, core: 2. Of those that a mesh axis runs over, the one named last changes fastest.
Arguments:
- tokens: bfloat16 [256, 4096], P('dp', 'tp'), may hold values from -6 to 6
- lengths: int32 [256], P('dp'), may hold values from 1 to 96, 6144 in all
- norm_gain: float32 [2, 4096], replicated, may hold values from 0.1 to 1.9
- w_recept: bfloat16 [2, 4096, 4096], P(None, None, ('tp', 'dp')), may hold values from -0.09375 to 0.09375
- w_key: bfloat16 [2, 4096, 4096], P(None, None, ('tp', 'dp')), may hold values from -0.09375 to 0.09375
- w_value: bfloat16 [2, 4096, 4096], P(None, None, ('tp', 'dp')), may hold values from -0.09375 to 0.09375
- w_decay: bfloat16 [2, 4096, 4096], P(None, None, ('tp', 'dp')), may hold values from -0.09375 to 0.09375
- w_rate: bfloat16 [2, 4096, 4096], P(None, None, ('tp', 'dp')), may hold values from -0.09375 to 0.09375
- w_gate: bfloat16 [2, 4096, 4096], P(None, None, ('tp', 'dp')), may hold values from -0.09375 to 0.09375
- w_out: bfloat16 [2, 4096, 4096], P(None, None, ('tp', 'dp')), may hold values from -0.09375 to 0.09375
- decay_base: float32 [2, 4096], P(None, 'tp'), may hold values from -3 to 1
- rate_base: float32 [2, 4096], P(None, 'tp'), may hold values from -3 to 3
- group_gain: float32 [2, 4096], P(None, 'tp'), may hold values from 0.1 to 1.9
- state: float32 [2, 256, 64, 64, 64], P(None, 'dp', 'tp'), may hold values from -6 to 6
Outputs:
- mixed: bfloat16 [256, 4096], P('dp', 'tp')
- new_state: float32 [2, 256, 64, 64, 64], P(None, 'dp', 'tp')
Inputs may be any that keep to these rules, and one draw needn't show every extreme that they name: Each sequence's live length lies between 1 and 96, some sequences reach 96, and the lengths sum to 6144.
All inputs are finite; a program needn't handle non-finite values.
Results may differ from a plain program's by a relative error of at most 0.025.
Values may be sent and summed in bfloat16 or wider, within the bound.
A program may use at most 128 MiB of HBM per device.

v0:
```python
import functools

import jax
import jax.numpy as jnp
from jax import lax
from jax.experimental import pallas as pl
from jax.experimental.pallas import tpu as pltpu
from jax.sharding import PartitionSpec as P

STEP = 16
RMS_EPS = 1e-06
GROUP_EPS = 0.00064
VMEM_LIMIT = 56 * 1024 * 1024


MESH = pl.DeviceIdType.MESH


def greet(peers):
    barrier = pltpu.get_barrier_semaphore()
    for tp, dp in peers:
        pl.semaphore_signal(barrier, inc=1, device_id=(tp, dp), device_id_type=MESH)
    pl.semaphore_wait(barrier, len(peers))


def gather_body(x_ref, out_ref, own_sem, send_sem, recv_sem, *, tp, dp):
    t, d = lax.axis_index("tp"), lax.axis_index("dp")
    core = lax.rem(d, 2)
    sibling = d + 1 - 2 * core
    others = [lax.rem(d + 2 * k, dp) for k in range(1, dp // 2)]
    sent = []

    def send(source, slot, to_t, to_d):
        copy = pltpu.make_async_remote_copy(
            src_ref=source,
            dst_ref=out_ref.at[slot],
            send_sem=send_sem.at[len(sent)],
            recv_sem=recv_sem.at[slot],
            device_id=(to_t, to_d),
            device_id_type=MESH,
        )
        copy.start()
        sent.append(copy)

    def arrived(slot):
        pltpu.make_async_remote_copy(
            src_ref=x_ref,
            dst_ref=out_ref.at[slot],
            send_sem=send_sem.at[0],
            recv_sem=recv_sem.at[slot],
            device_id=(t, sibling),
            device_id_type=MESH,
        ).wait_recv()

    rows = [lax.rem(t + k, tp) for k in range(1, tp)]
    greet([(r, d) for r in rows] + [(t, o) for o in others] + [(t, sibling)])
    mine = t * dp + d
    own = pltpu.make_async_copy(x_ref, out_ref.at[mine], own_sem)
    own.start()
    for r in rows:
        send(x_ref, mine, r, d)
    for o in others + [sibling]:
        send(x_ref, mine, t, o)
    for k in range(1, tp):
        slot = lax.rem(t + tp - k, tp) * dp + d
        arrived(slot)
        for o in others + [sibling]:
            send(out_ref.at[slot], slot, t, o)
    for k in range(tp):
        for o in others:
            slot = lax.rem(t + tp - k, tp) * dp + o
            arrived(slot)
            send(out_ref.at[slot], slot, t, sibling)
    for k in range(tp):
        for o in [d] + others:
            arrived(lax.rem(t + tp - k, tp) * dp + o + sibling - d)
    own.wait()
    for copy in sent:
        copy.wait_send()


def gather(x, tp, dp, number):
    count = (tp - 1) + tp * (dp // 2) + tp * (dp // 2 - 1)
    return pl.pallas_call(
        functools.partial(gather_body, tp=tp, dp=dp),
        out_shape=jax.ShapeDtypeStruct((tp * dp,) + x.shape, x.dtype),
        in_specs=[pl.BlockSpec(memory_space=pltpu.VMEM)],
        out_specs=pl.BlockSpec(memory_space=pltpu.VMEM),
        scratch_shapes=[
            pltpu.SemaphoreType.DMA,
            pltpu.SemaphoreType.DMA((count,)),
            pltpu.SemaphoreType.DMA((tp * dp,)),
        ],
        compiler_params=pltpu.CompilerParams(collective_id=number, has_side_effects=True),
        name="gather",
    )(x)


def exchange_body(x_ref, out_ref, own_sem, send_sem, recv_sem, *, dp):
    t, d = lax.axis_index("tp"), lax.axis_index("dp")
    peers = [lax.rem(d + k, dp) for k in range(1, dp)]
    greet([(t, o) for o in peers])
    own = pltpu.make_async_copy(x_ref.at[d], out_ref.at[d], own_sem)
    own.start()
    sent = []
    for k, o in enumerate(peers):
        copy = pltpu.make_async_remote_copy(
            src_ref=x_ref.at[o],
            dst_ref=out_ref.at[d],
            send_sem=send_sem.at[k],
            recv_sem=recv_sem.at[k],
            device_id=(t, o),
            device_id_type=MESH,
        )
        copy.start()
        sent.append(copy)
    for k in range(1, dp):
        source = lax.rem(d + dp - k, dp)
        pltpu.make_async_remote_copy(
            src_ref=x_ref.at[source],
            dst_ref=out_ref.at[source],
            send_sem=send_sem.at[k - 1],
            recv_sem=recv_sem.at[k - 1],
            device_id=(t, source),
            device_id_type=MESH,
        ).wait_recv()
    own.wait()
    for copy in sent:
        copy.wait_send()


def exchange(x, dp, number):
    return pl.pallas_call(
        functools.partial(exchange_body, dp=dp),
        out_shape=jax.ShapeDtypeStruct(x.shape, x.dtype),
        in_specs=[pl.BlockSpec(memory_space=pltpu.VMEM)],
        out_specs=pl.BlockSpec(memory_space=pltpu.VMEM),
        scratch_shapes=[
            pltpu.SemaphoreType.DMA,
            pltpu.SemaphoreType.DMA((dp - 1,)),
            pltpu.SemaphoreType.DMA((dp - 1,)),
        ],
        compiler_params=pltpu.CompilerParams(collective_id=number, has_side_effects=True),
        name="exchange",
    )(x)


def joined_block(x_ref, across):
    if across:
        return jnp.concatenate([x_ref[j] for j in range(x_ref.shape[0])], axis=1)
    return x_ref[...].reshape(x_ref.shape[0] * x_ref.shape[1], x_ref.shape[2])


def project_body(x_ref, gain_ref, *refs, features, steps, across):
    weights, out_ref, acc, square = refs[:6], refs[6], refs[7], refs[8]
    step = pl.program_id(0)
    slim = weights[0].shape[-1]

    @pl.when(step == 0)
    def _():
        acc[...] = jnp.zeros_like(acc)
        square[...] = jnp.zeros_like(square)

    values = joined_block(x_ref, across).astype(jnp.float32)
    square[...] += jnp.sum(values * values, axis=1, keepdims=True)
    scaled = (values * gain_ref[...]).astype(jnp.bfloat16)
    if slim % 128 == 0:
        joined = jnp.concatenate([w[0] for w in weights], axis=1)
        total = jnp.dot(scaled, joined, preferred_element_type=jnp.float32)
        for idx in range(6):
            acc[idx] += total[:, idx * slim : (idx + 1) * slim]
    else:
        for idx in range(6):
            acc[idx] += jnp.dot(scaled, weights[idx][0], preferred_element_type=jnp.float32)

    @pl.when(step == steps - 1)
    def _():
        factor = lax.rsqrt(square[...] / features + RMS_EPS)
        for idx in range(6):
            done = (acc[idx] * factor).astype(out_ref.dtype)
            share = out_ref.shape[2]
            for j in range(out_ref.shape[0]):
                out_ref[j, idx] = done[j * share : (j + 1) * share]


def project(x, gain, weights, layer, steps, dp, across):
    features, slim = weights[0].shape[1:]
    part = x.shape[0] // steps
    depth = features // steps
    rows = x.shape[1] * (1 if across else part)
    return pl.pallas_call(
        functools.partial(project_body, features=features, steps=steps, across=across),
        grid=(steps,),
        out_shape=jax.ShapeDtypeStruct((dp, 6, rows // dp, slim), jnp.bfloat16),
        in_specs=[
            pl.BlockSpec((part,) + x.shape[1:], lambda i: (i, 0, 0)),
            pl.BlockSpec((1, depth), lambda i: (0, i)),
        ]
        + [pl.BlockSpec((1, depth, slim), lambda i: (layer, i, 0))] * 6,
        out_specs=pl.BlockSpec((dp, 6, rows // dp, slim), lambda i: (0, 0, 0, 0)),
        scratch_shapes=[
            pltpu.VMEM((6, rows, slim), jnp.float32),
            pltpu.VMEM((rows, 1), jnp.float32),
        ],
        compiler_params=pltpu.CompilerParams(vmem_limit_bytes=VMEM_LIMIT),
        name="project",
    )(x, gain, *weights)


def fold_body(x_ref, w_ref, out_ref, acc, *, steps):
    step = pl.program_id(0)

    @pl.when(step == 0)
    def _():
        acc[...] = jnp.zeros_like(acc)

    acc[...] += jnp.dot(joined_block(x_ref, False), w_ref[0], preferred_element_type=jnp.float32)

    @pl.when(step == steps - 1)
    def _():
        out_ref[...] = acc[...].astype(out_ref.dtype)


def fold(x, weight, layer, steps):
    features, slim = weight.shape[1:]
    part = x.shape[0] // steps
    depth = features // steps
    rows = part * x.shape[1]
    return pl.pallas_call(
        functools.partial(fold_body, steps=steps),
        grid=(steps,),
        out_shape=jax.ShapeDtypeStruct((rows, slim), jnp.bfloat16),
        in_specs=[
            pl.BlockSpec((part,) + x.shape[1:], lambda i: (i, 0, 0)),
            pl.BlockSpec((1, depth, slim), lambda i: (layer, i, 0)),
        ],
        out_specs=pl.BlockSpec((rows, slim), lambda i: (0, 0)),
        scratch_shapes=[pltpu.VMEM((rows, slim), jnp.float32)],
        compiler_params=pltpu.CompilerParams(vmem_limit_bytes=VMEM_LIMIT),
        name="fold",
    )(x, weight)


def recur_body(vec_ref, lens_ref, base_ref, rate_ref, gain_ref, state_ref, *refs):
    new_ref, mixed_ref, rows_s, read_s = refs[-4:]
    group, heads, size = state_ref.shape[1], state_ref.shape[2], state_ref.shape[3]
    live = lens_ref[...] > STEP
    for h in range(heads):
        part = slice(h * size, (h + 1) * size)
        recept, key, value, decay_pre, rate_pre = [
            vec_ref[q, :, part].astype(jnp.float32) for q in range(5)
        ]
        decay = jnp.exp(-jnp.exp(-jax.nn.softplus(-(base_ref[:, part] + decay_pre)) - 0.5))
        rate = jax.nn.sigmoid(rate_ref[:, part] + rate_pre)
        length = jnp.maximum(jnp.sqrt(jnp.sum(key * key, axis=1, keepdims=True)), 1e-12)
        unit = key / length
        rows_s[0, h] = -unit
        rows_s[1, h] = value * length
        rows_s[2, h] = decay
        rows_s[3, h] = unit * rate
        rows_s[4, h] = recept
    across = lax.broadcasted_iota(jnp.int32, (size, size), 0)
    along = lax.broadcasted_iota(jnp.int32, (size, size), 1)
    eye = across == along

    def one(b, carry):
        keep = lens_ref[pl.ds(b, 1), :size] > STEP
        for h in range(heads):
            neg, held, decay, rated, recept = [rows_s[q, h, pl.ds(b, 1), :] for q in range(5)]
            old = state_ref[0, b, h]
            terms = old * neg + jnp.where(eye, held, 0.0)
            weight = jnp.sum(terms, axis=1, keepdims=True)
            updated = old * decay + weight * rated
            new_ref[0, b, h] = jnp.where(keep, updated, old)
            read = jnp.sum(updated * recept, axis=1, keepdims=True)
            read_s[h, pl.ds(b, 1), :] = jnp.sum(jnp.where(eye, read, 0.0), axis=0, keepdims=True)
        return carry

    lax.fori_loop(0, group, one, 0)
    for h in range(heads):
        part = slice(h * size, (h + 1) * size)
        read = read_s[h]
        centre = jnp.mean(read, axis=1, keepdims=True)
        apart = read - centre
        spread = jnp.mean(apart * apart, axis=1, keepdims=True)
        normal = apart * lax.rsqrt(spread + GROUP_EPS) * gain_ref[:, part]
        gate = jax.nn.sigmoid(vec_ref[5, :, part].astype(jnp.float32))
        mixed_ref[:, part] = jnp.where(live[:, :size], normal * gate, 0.0).astype(mixed_ref.dtype)


def recur(vec, lens, base, rate, gain, state, earlier, layer):
    _, rows, width = vec.shape
    heads, size = state.shape[2], state.shape[3]
    group = 8
    block = pl.BlockSpec((1, group, heads, size, size), lambda i: (layer, i, 0, 0, 0))
    line = pl.BlockSpec((1, width), lambda i: (0, 0))
    operands = [vec, lens, base, rate, gain, state]
    in_specs = [
        pl.BlockSpec((6, group, width), lambda i: (0, i, 0)),
        pl.BlockSpec((group, lens.shape[1]), lambda i: (i, 0)),
        line,
        line,
        line,
        block,
    ]
    aliases = {}
    if earlier is not None:
        operands.append(earlier)
        in_specs.append(pl.BlockSpec(memory_space=pl.ANY))
        aliases = {6: 0}
    return pl.pallas_call(
        recur_body,
        grid=(rows // group,),
        out_shape=(
            jax.ShapeDtypeStruct(state.shape, state.dtype),
            jax.ShapeDtypeStruct((rows, width), jnp.bfloat16),
        ),
        in_specs=in_specs,
        out_specs=(block, pl.BlockSpec((group, width), lambda i: (i, 0))),
        scratch_shapes=[
            pltpu.VMEM((5, heads, group, size), jnp.float32),
            pltpu.VMEM((heads, group, size), jnp.float32),
        ],
        input_output_aliases=aliases,
        compiler_params=pltpu.CompilerParams(vmem_limit_bytes=VMEM_LIMIT),
        name="recur",
    )(*operands)


def on_device(
    tokens,
    lengths,
    norm_gain,
    w_recept,
    w_key,
    w_value,
    w_decay,
    w_rate,
    w_gate,
    w_out,
    decay_base,
    rate_base,
    group_gain,
    state,
):
    weights = (w_recept, w_key, w_value, w_decay, w_rate, w_gate)
    tp, dp = lax.axis_size("tp"), lax.axis_size("dp")
    rows, slim = lengths.shape[0], w_out.shape[2]
    lens = jnp.broadcast_to(lengths[:, None], (rows, 128))
    every, across = gather(tokens, tp, dp, 0), False
    states = None
    for layer in range(2):
        pick = slice(layer, layer + 1)
        pieces = project(every, norm_gain[pick], weights, layer, tp, dp, across)
        vec = exchange(pieces, dp, 1 + layer)
        vec = vec.transpose(1, 2, 0, 3).reshape(6, rows, dp * slim)
        states, mixed = recur(
            vec, lens, decay_base[pick], rate_base[pick], group_gain[pick], state, states, layer
        )
        columns = fold(gather(mixed, tp, dp, 3 + layer), w_out, layer, tp)
        if layer == 0:
            across = slim % 128 == 0
            if across:
                every = gather(columns, tp, dp, 5)
            else:
                every = lax.all_gather(columns, ("tp", "dp"), axis=1, tiled=True)
                every = every.reshape(dp * rows, tp, dp * slim).transpose(1, 0, 2)
    current = exchange(columns.reshape(dp, rows, slim), dp, 6)
    return (current.transpose(1, 0, 2).reshape(rows, dp * slim), states)


def solution(mesh):
    in_specs = (
        P("dp", "tp"),
        P("dp"),
        P(),
        P(None, None, ("tp", "dp")),
        P(None, None, ("tp", "dp")),
        P(None, None, ("tp", "dp")),
        P(None, None, ("tp", "dp")),
        P(None, None, ("tp", "dp")),
        P(None, None, ("tp", "dp")),
        P(None, None, ("tp", "dp")),
        P(None, "tp"),
        P(None, "tp"),
        P(None, "tp"),
        P(None, "dp", "tp", None, None),
    )
    out_specs = (P("dp", "tp"), P(None, "dp", "tp", None, None))
    return jax.shard_map(
        on_device, mesh=mesh, in_specs=in_specs, out_specs=out_specs, check_vma=False
    )
```

profile of v0, /device:TPU:0, one launch (start us, length us, event | category | flops | bytes accessed | tf_op | source)
XLA Modules:
  0.0 277.1 jit_solution(10263805842390965121)
XLA Ops:
  7.2 1.3 fusion.3
  8.6 1.5 fusion
  10.0 2.7 copy.52.refs_0_
  12.8 1.8 copy.53.refs_1_
  14.5 1.8 copy.54.refs_2_
  16.3 1.8 copy.55.refs_3_
  18.1 1.8 copy.56.refs_4_
  19.9 1.7 copy.57.refs_5_
  21.6 1.7 copy.59.w_ref
  23.4 27.9 %gather.3.x_ref = bf16[128,32,256]{2,1,0:T(8,128)(2,1)} custom-call(bf16[32,256]{1,0:T(8,128)(2,1)} %x_ref.1), custom_call_target="tpu_custom_call" | custom-call | tf_op jit(solution)/shard_map/gather/pallas_call | solution.py:84
  51.3 12.8 %project.2.x_ref = bf16[8,6,32,32]{3,2,1,0:T(8,128)(2,1)} custom-call(bf16[128,32,256]{2,1,0:T(8,128)(2,1)} %gather.3.x_ref, f32[1,4096]{1,0:T(1,128)} %get-tuple-element.11.gain_ref, bf16[2,4096,32]{2,1,0:T(8,128)(2,1)} %copy.52.refs_0_, bf16[2,4096,32]{2,1,0:T(8,128)(2,1)} %copy.53.refs_1_, bf16[2,4096,32]{2,1,0:T(8,128)(2,1)} %copy.54.refs_2_, ...), custom_call_target="tpu_custom_call" | custom-call | tf_op jit(solution)/shard_map/project/pallas_call | solution.py:191
  64.1 10.3 %exchange.3 = bf16[8,6,32,32]{3,2,1,0:T(8,128)(2,1)} custom-call(bf16[8,6,32,32]{3,2,1,0:T(8,128)(2,1)} %project.2.x_ref), custom_call_target="tpu_custom_call" | custom-call | tf_op jit(solution)/shard_map/exchange/pallas_call | solution.py:133
  77.9 10.4 %recur.2 = (f32[2,32,4,64,64]{4,3,2,1,0:T(8,128)}, bf16[32,256]{1,0:T(8,128)(2,1)}) custom-call(bf16[6,32,256]{2,1,0:T(8,128)(2,1)} %reshape.20.vec_ref, s32[32,128]{1,0:T(8,128)} %broadcast_in_dim.2.lens_ref, f32[1,256]{1,0:T(1,128)} %get-tuple-element.17.base_ref, f32[1,256]{1,0:T(1,128)} %get-tuple-element.18.rate_ref, ...), custom_call_target="tpu_custom_call" | custom-call | tf_op jit(solution)/shard_map/recur/pallas_call | solution.py:311
  88.2 25.4 %gather.4.x_ref = bf16[128,32,256]{2,1,0:T(8,128)(2,1)} custom-call(bf16[32,256]{1,0:T(8,128)(2,1)} %get-tuple-element.6.x_ref), custom_call_target="tpu_custom_call" | custom-call | tf_op jit(solution)/shard_map/gather/pallas_call | solution.py:84
  113.6 9.7 %fold.2 = bf16[256,32]{1,0:T(8,128)(2,1)} custom-call(bf16[128,32,256]{2,1,0:T(8,128)(2,1)} %gather.4.x_ref, bf16[2,4096,32]{2,1,0:T(8,128)(2,1)} %copy.59.w_ref), custom_call_target="tpu_custom_call" | custom-call | tf_op jit(solution)/shard_map/fold/pallas_call | solution.py:229
  123.3 1.5 copy.60
  124.9 62.6 %all-gather.2.cloned.1.call-done = bf16[256,4096]{0,1:T(8,128)(2,1)} async-done(((bf16[256,32]{0,1:T(8,128)(2,1)}), bf16[256,4096]{0,1:T(8,128)(2,1)}) %all-gather.2.cloned.1.call-update) | async-done | bytes 2097168 | tf_op jit(solution)/shard_map/all_gather | solution.py:366
  187.4 3.9 %copy.61 = bf16[256,16,256]{2,0,1:T(8,128)(2,1)} copy(bf16[256,16,256]{0,2,1:T(8,128)(2,1)} %bitcast.11) | data formatting | bytes 4194304 | tf_op jit(solution)/shard_map/reshape | solution.py:367
  191.4 12.9 %project.3.x_ref = bf16[8,6,32,32]{3,2,1,0:T(8,128)(2,1)} custom-call(bf16[16,256,256]{2,1,0:T(8,128)(2,1)} %bitcast.10, f32[1,4096]{1,0:T(1,128)} %get-tuple-element.10.gain_ref, bf16[2,4096,32]{2,1,0:T(8,128)(2,1)} %copy.52.refs_0_, bf16[2,4096,32]{2,1,0:T(8,128)(2,1)} %copy.53.refs_1_, bf16[2,4096,32]{2,1,0:T(8,128)(2,1)} %copy.54.refs_2_, ...), custom_call_target="tpu_custom_call" | custom-call | tf_op jit(solution)/shard_map/project/pallas_call | solution.py:191
  204.2 10.1 %exchange.4 = bf16[8,6,32,32]{3,2,1,0:T(8,128)(2,1)} custom-call(bf16[8,6,32,32]{3,2,1,0:T(8,128)(2,1)} %project.3.x_ref), custom_call_target="tpu_custom_call" | custom-call | tf_op jit(solution)/shard_map/exchange/pallas_call | solution.py:133
  216.6 10.4 %recur.3 = (f32[2,32,4,64,64]{4,3,2,1,0:T(8,128)}, bf16[32,256]{1,0:T(8,128)(2,1)}) custom-call(bf16[6,32,256]{2,1,0:T(8,128)(2,1)} %reshape.22.vec_ref, s32[32,128]{1,0:T(8,128)} %broadcast_in_dim.2.lens_ref, f32[1,256]{1,0:T(1,128)} %get-tuple-element.16.base_ref, f32[1,256]{1,0:T(1,128)} %get-tuple-element.19.rate_ref, ...), custom_call_target="tpu_custom_call", output_to_operand_aliasing={{0}: (6, {})} | custom-call | tf_op jit(solution)/shard_map/recur/pallas_call | solution.py:311
  227.0 24.9 %gather.5.x_ref = bf16[128,32,256]{2,1,0:T(8,128)(2,1)} custom-call(bf16[32,256]{1,0:T(8,128)(2,1)} %get-tuple-element.8.x_ref), custom_call_target="tpu_custom_call" | custom-call | tf_op jit(solution)/shard_map/gather/pallas_call | solution.py:84
  251.9 9.7 %fold.3 = bf16[256,32]{1,0:T(8,128)(2,1)} custom-call(bf16[128,32,256]{2,1,0:T(8,128)(2,1)} %gather.5.x_ref, bf16[2,4096,32]{2,1,0:T(8,128)(2,1)} %copy.59.w_ref), custom_call_target="tpu_custom_call" | custom-call | tf_op jit(solution)/shard_map/fold/pallas_call | solution.py:229
  261.6 7.1 %exchange.5 = bf16[8,32,32]{2,1,0:T(8,128)(2,1)} custom-call(bf16[8,32,32]{2,1,0:T(8,128)(2,1)} %bitcast.14), custom_call_target="tpu_custom_call" | custom-call | tf_op jit(solution)/shard_map/exchange/pallas_call | solution.py:133
  (28 shorter events, 7.3 us)
Async XLA Ops:
  7.2 5.6 %copy-start = (bf16[2,4096,32]{1,2,0:T(8,128)(2,1)S(1)}, bf16[2,4096,32]{1,2,0:T(8,128)(2,1)}, u32[]{:S(2)}) copy-start(bf16[2,4096,32]{1,2,0:T(8,128)(2,1)} %param.18) | copy-start | bytes 1572868
  7.2 180.3 %all-gather.2.cloned.1.call-start = ((), (), s32[]{:S(2)}) async-start(), calls=%async_computation | async-start | bytes 2113536 | tf_op jit(solution)/shard_map/all_gather | solution.py:366
  10.0 4.5 %copy-start.1 = (bf16[2,4096,32]{1,2,0:T(8,128)(2,1)S(1)}, bf16[2,4096,32]{1,2,0:T(8,128)(2,1)}, u32[]{:S(2)}) copy-start(bf16[2,4096,32]{1,2,0:T(8,128)(2,1)} %param.19) | copy-start | bytes 1572868
  12.8 3.6 %copy-start.2 = (bf16[2,4096,32]{1,2,0:T(8,128)(2,1)S(1)}, bf16[2,4096,32]{1,2,0:T(8,128)(2,1)}, u32[]{:S(2)}) copy-start(bf16[2,4096,32]{1,2,0:T(8,128)(2,1)} %param.20) | copy-start | bytes 1572868
  14.5 3.6 %copy-start.3 = (bf16[2,4096,32]{1,2,0:T(8,128)(2,1)S(1)}, bf16[2,4096,32]{1,2,0:T(8,128)(2,1)}, u32[]{:S(2)}) copy-start(bf16[2,4096,32]{1,2,0:T(8,128)(2,1)} %param.21) | copy-start | bytes 1572868
  16.3 3.5 %copy-start.4 = (bf16[2,4096,32]{1,2,0:T(8,128)(2,1)S(1)}, bf16[2,4096,32]{1,2,0:T(8,128)(2,1)}, u32[]{:S(2)}) copy-start(bf16[2,4096,32]{1,2,0:T(8,128)(2,1)} %param.22) | copy-start | bytes 1572868
  18.1 3.5 %copy-start.5 = (bf16[2,4096,32]{1,2,0:T(8,128)(2,1)S(1)}, bf16[2,4096,32]{1,2,0:T(8,128)(2,1)}, u32[]{:S(2)}) copy-start(bf16[2,4096,32]{1,2,0:T(8,128)(2,1)} %param.23) | copy-start | bytes 1572868
  51.3 25.3 %copy-start.6 = (f32[2,256]{1,0:T(2,128)S(1)}, f32[2,256]{1,0:T(2,128)}, u32[]{:S(2)}) copy-start(f32[2,256]{1,0:T(2,128)} %param.26) | copy-start | bytes 6148
  51.3 25.3 %copy-start.7 = (f32[2,256]{1,0:T(2,128)S(1)}, f32[2,256]{1,0:T(2,128)}, u32[]{:S(2)}) copy-start(f32[2,256]{1,0:T(2,128)} %param.25) | copy-start | bytes 6148
  51.3 25.9 %copy-start.8 = (s32[32]{0:T(128)S(1)}, s32[32]{0:T(128)}, u32[]{:S(2)}) copy-start(s32[32]{0:T(128)} %param.15) | copy-start | bytes 388
Sparse Core Ops, SparseCore 0:
  125.0 62.3 all-gather.1
where the time goes:
time: 280 us; the launch traced here: 277 us
  Pallas kernels  172 us (61%)
  waiting for transfers between devices  62.6 us (22%)
  local copies, waits for them, and re-layouts  28.8 us (10%)
  between operations  14.1 us (5%)
    pallas_call x3, Pallas kernels, gather(): pl.pallas_call(functools.partial(gather_body, tp=tp, dp=dp), out_shape=ja...  78.2 us
    all_gather x1, waiting for transfers between devices, on_device(): every = lax.all_gather(columns, ('tp', 'dp'), axis=1, tiled=True)  62.6 us
    pallas_call x3, Pallas kernels, exchange(): pl.pallas_call(functools.partial(exchange_body, dp=dp), out_shape=jax.Sha...  27.5 us
    pallas_call x2, Pallas kernels, project(): pl.pallas_call(functools.partial(project_body, features=features, steps=s...  25.7 us
    pallas_call x2, Pallas kernels, recur(): pl.pallas_call(recur_body, grid=(rows // group,), out_shape=(jax.ShapeDty...  20.7 us
    pallas_call x2, Pallas kernels, fold(): pl.pallas_call(functools.partial(fold_body, steps=steps), grid=(steps,),...  19.4 us
    unnamed x25, local copies, waits for them, and re-layouts  13.3 us
  transfers between devices with their start and end apart: 1, of which 1 were waited for; matrix products, arithmetic and copies ran while one was open for 0% of the time, Pallas kernels for 0%

commit v1 on v0

v1 whole, which is shorter than its diff:
```python
import functools

import jax
import jax.numpy as jnp
from jax import lax
from jax.experimental import pallas as pl
from jax.experimental.pallas import tpu as pltpu
from jax.sharding import PartitionSpec as P

STEP = 16
RMS_EPS = 1e-06
GROUP_EPS = 0.00064
VMEM_LIMIT = 56 * 1024 * 1024
MESH = pl.DeviceIdType.MESH


def dot_t(a, b):
    return lax.dot_general(a, b, (((1,), (1,)), ((), ())), preferred_element_type=jnp.float32)


def plane_offsets(tp):
    ny = 4 if tp == 16 else tp
    nz = tp // ny
    hops = lambda k, n: min(k, n - k)
    offs = [(dz, dy) for dz in range(nz) for dy in range(ny)]
    offs.sort(key=lambda o: (hops(o[0], nz) + hops(o[1], ny), o))
    return ny, nz, offs


def step_body(
    tok, lens, gain, base, rate, ggain, wr, wk, wv, wd, wa, wg, wo, state,
    mixed_ref, rows_ref,
    xg, wcat, wot, vg, mg, pieces, st, acc, square,
    ag_send, a1_recv, b1_recv, fin_recv, ex_send, ex_recv, mg_send, mg_recv,
    wo_send, wo_recv, wc_send, wc_recv, own_sem, st_sem,
    *, tp, dp,
):
    t, d = lax.axis_index("tp"), lax.axis_index("dp")
    nx = dp // 2
    x, core = d // 2, lax.rem(d, 2)
    sibling = d + 1 - 2 * core
    ny, nz, offs = plane_offsets(tp)
    z, y = t // ny, lax.rem(t, ny)
    rows, width = tok.shape
    slim = width // dp
    feat = tp * width
    half = rows // 2
    weights = (wr, wk, wv, wd, wa, wg)

    def plane(off):
        return lax.rem(z + off[0], nz) * ny + lax.rem(y + off[1], ny)

    def xpeer(k):
        return lax.rem(x + k + nx, nx)

    def remote(src, dst, ssem, rsem, tt, dd):
        return pltpu.make_async_remote_copy(
            src_ref=src, dst_ref=dst, send_sem=ssem, recv_sem=rsem,
            device_id=(tt, dd), device_id_type=MESH,
        )

    def arrived(ref, sem):
        remote(ref, ref, ag_send.at[0], sem, t, sibling).wait_recv()

    peers = [plane(o) for o in offs[1:]]
    far = peers[::-1]
    ks = [1, nx - 1] + list(range(2, nx - 1))
    xs = [xpeer(k) for k in ks]

    local = []

    def fetch(src, dst, sem):
        copy = pltpu.make_async_copy(src, dst, sem)
        copy.start()
        return copy

    def wrow(q):
        return pl.ds(pl.multiple_of(q * 2 * slim + core * slim, slim), slim)

    def worow(dd, start=0, count=None):
        return pl.ds(pl.multiple_of(dd * slim + start, slim // 2), slim if count is None else count)

    own_w = [[fetch(weights[q].at[l], wcat.at[l, wrow(q)], own_sem.at[l, q]) for q in range(6)] for l in range(2)]
    own_o = [fetch(wo.at[l], wot.at[l, worow(d)], own_sem.at[l, 6]) for l in range(2)]
    own_s = [fetch(state.at[l], st.at[l], st_sem.at[l]) for l in range(2)]

    barrier = pltpu.get_barrier_semaphore()
    everyone = [(p, d) for p in far] + [(t, 2 * o + core) for o in xs] + [(t, sibling)]
    for p in everyone:
        pl.semaphore_signal(barrier, inc=1, device_id=p, device_id_type=MESH)
    pl.semaphore_wait(barrier, len(everyone))

    def own_rows(h, xx):
        return pl.ds(pl.multiple_of(xx * rows + h * half, half), half)

    def gather_start(l, source):
        sent = []

        def send(src, dst, rsem, tt, dd):
            copy = remote(src, dst, ag_send.at[len(sent)], rsem, tt, dd)
            copy.start()
            sent.append(copy)

        a_dst, b_dst = xg.at[l, t, own_rows(0, x)], xg.at[l, t, own_rows(1, x)]
        for o in xs:
            send(source(0), a_dst, a1_recv.at[l, x], t, 2 * o + core)
        for p in far:
            send(source(1), b_dst, b1_recv.at[l, t], p, d)
        for p in far:
            send(source(0), a_dst, fin_recv.at[l, t], p, d)
        for o in xs:
            send(source(1), b_dst, fin_recv.at[l, t], t, 2 * o + core)
        return sent, send

    def gather_relay(l, send):
        for o in xs:
            block = xg.at[l, t, own_rows(0, o)]
            arrived(block, a1_recv.at[l, o])
            for p in far:
                send(block, block, fin_recv.at[l, t], p, d)
        for p in peers:
            block = xg.at[l, p, own_rows(1, x)]
            arrived(block, b1_recv.at[l, p])
            for o in xs:
                send(block, block, fin_recv.at[l, p], t, 2 * o + core)

    def prepare(l):
        for q in range(6):
            own_w[l][q].wait()
        for q in range(6):
            other = pl.ds(pl.multiple_of(q * 2 * slim + (1 - core) * slim, slim), slim)
            arrived(wcat.at[l, other], wc_recv.at[l, q])
        line = gain[l : l + 1, :]

        def one(i, carry):
            part = pl.ds(pl.multiple_of(i * 16, 16), 16)
            wcat[l, part, :] = (wcat[l, part, :].astype(jnp.float32) * line).astype(jnp.bfloat16)
            return carry

        lax.fori_loop(0, 12 * slim // 16, one, 0)

    def project(l):
        acc[...] = jnp.zeros_like(acc)
        square[...] = jnp.zeros_like(square)
        for o in offs:
            tt = plane(o)
            count = (nx - 1) * half if o == (0, 0) else (2 * nx - 1) * half
            arrived(xg.at[l, tt, pl.ds(0, count)], fin_recv.at[l, tt])
            block = xg[l, tt]
            cols = pl.ds(pl.multiple_of(tt * width, width), width)
            acc[...] += dot_t(block, wcat[l, :, cols])
            values = block.astype(jnp.float32)
            values = values * values
            total = values[:, :128]
            for j in range(1, width // 128):
                total += values[:, j * 128 : (j + 1) * 128]
            square[...] += total
        factor = lax.rsqrt(jnp.sum(square[...], axis=1, keepdims=True) / feat + RMS_EPS)
        done = (acc[...] * factor).astype(jnp.bfloat16)
        for j in range(nx):
            pieces[l, j] = done[j * rows : (j + 1) * rows]
        sent = []
        for i, o in enumerate(xs):
            copy = remote(pieces.at[l, o], vg.at[l, x], ex_send.at[l, i], ex_recv.at[l, x], t, 2 * o + core)
            copy.start()
            sent.append(copy)
        vg[l, x] = pieces[l, x]
        return sent

    def out_slot(l, xx, cc, start=0, count=None):
        return wot.at[l, worow(2 * xx + cc, start, count)]

    def out_start(l):
        own_o[l].wait()
        up, down = xpeer(1), xpeer(-1)
        block = out_slot(l, x, core)
        sent = [
            remote(block, block, wo_send.at[l, 0], wo_recv.at[l, 0], t, 2 * up + core),
            remote(block, block, wo_send.at[l, 1], wo_recv.at[l, 1], t, 2 * down + core),
            remote(block, block, wo_send.at[l, 2], wo_recv.at[l, 4], t, sibling),
        ]
        for copy in sent:
            copy.start()
        return sent

    def out_relay(l, sent):
        up, down, across = xpeer(1), xpeer(-1), xpeer(2)
        part = slim // 2
        below, above = out_slot(l, down, core), out_slot(l, up, core)
        arrived(below, wo_recv.at[l, 0])
        first = out_slot(l, down, core, 0, part)
        one = remote(first, first, wo_send.at[l, 3], wo_recv.at[l, 2], t, 2 * up + core)
        one.start()
        two = remote(below, below, wo_send.at[l, 4], wo_recv.at[l, 5], t, sibling)
        two.start()
        arrived(above, wo_recv.at[l, 1])
        second = out_slot(l, up, core, part, part)
        three = remote(second, second, wo_send.at[l, 5], wo_recv.at[l, 3], t, 2 * down + core)
        three.start()
        four = remote(above, above, wo_send.at[l, 6], wo_recv.at[l, 6], t, sibling)
        four.start()
        sent += [one, two, three, four]

    def out_finish(l, sent):
        up, down, across = xpeer(1), xpeer(-1), xpeer(2)
        part = slim // 2
        arrived(out_slot(l, across, core, 0, part), wo_recv.at[l, 2])
        arrived(out_slot(l, across, core, part, part), wo_recv.at[l, 3])
        block = out_slot(l, across, core)
        copy = remote(block, block, wo_send.at[l, 7], wo_recv.at[l, 7], t, sibling)
        copy.start()
        sent.append(copy)
        for i, xx in enumerate((x, down, up, across)):
            arrived(out_slot(l, xx, 1 - core), wo_recv.at[l, 4 + i])

    size = 2 * slim
    sub = lax.broadcasted_iota(jnp.int32, (rows, rows), 0)
    lane = lax.broadcasted_iota(jnp.int32, (rows, rows), 1)
    spread = jnp.where(sub == lane, lens[...].astype(jnp.float32), 0.0)
    live = jnp.sum(spread, axis=1, keepdims=True) > STEP
    eight = lax.broadcasted_iota(jnp.int32, (8, size), 0)

    def recur(l):
        for o in xs:
            arrived(vg.at[l, o], ex_recv.at[l, o])
        own_s[l].wait()
        looks, extras, gates = [], [], []
        for h in range(nx):
            part = slice(h * size, (h + 1) * size)
            recept, key, value, decay_pre, rate_pre, gate_pre = [
                vg[l, h, :, q * size : (q + 1) * size].astype(jnp.float32) for q in range(6)
            ]
            decay = jnp.exp(-jnp.exp(-jax.nn.softplus(-(base[l : l + 1, part] + decay_pre)) - 0.5))
            learn = jax.nn.sigmoid(rate[l : l + 1, part] + rate_pre)
            length = jnp.maximum(jnp.sqrt(jnp.sum(key * key, axis=1, keepdims=True)), 1e-12)
            unit = key / length
            rated = unit * learn
            held = value * length
            rho = jnp.sum(rated * recept, axis=1, keepdims=True)
            rows_ref[l, 0, h] = jnp.where(live, -unit, 0.0)
            rows_ref[l, 1, h] = jnp.where(live, held, 0.0)
            rows_ref[l, 2, h] = jnp.where(live, decay, 1.0)
            rows_ref[l, 3, h] = rated
            looks.append(decay * recept - rho * unit)
            extras.append(rho * held)
            gates.append(jax.nn.sigmoid(gate_pre) * ggain[l : l + 1, part])
        sent = []
        for g in range(2):
            outs = []
            for h in range(nx):
                reads = []
                for k in range(half // 8):
                    low = g * half + k * 8
                    look = looks[h][low : low + 8]
                    read = extras[h][low : low + 8]
                    for b in range(8):
                        got = dot_t(look, st[l, low + b, h])
                        read += jnp.where(eight == b, got, 0.0)
                    reads.append(read)
                read = jnp.concatenate(reads, axis=0)
                span = slice(g * half, (g + 1) * half)
                centre = jnp.mean(read, axis=1, keepdims=True)
                apart = read - centre
                var = jnp.mean(apart * apart, axis=1, keepdims=True)
                normal = apart * lax.rsqrt(var + GROUP_EPS) * gates[h][span]
                outs.append(jnp.where(live[span], normal, 0.0).astype(jnp.bfloat16))
            span = pl.ds(g * half, half)
            mg[l, t, span, :] = jnp.concatenate(outs, axis=1)
            block = mg.at[l, t, span]
            for i, p in enumerate(far):
                copy = remote(block, block, mg_send.at[l, g * (tp - 1) + i], mg_recv.at[l, t], p, d)
                copy.start()
                sent.append(copy)
        return sent

    def fold(l):
        total = jnp.zeros((rows, width), jnp.float32)
        for o in offs:
            tt = plane(o)
            if o != (0, 0):
                arrived(mg.at[l, tt], mg_recv.at[l, tt])
            cols = pl.ds(pl.multiple_of(tt * width, width), width)
            total += dot_t(mg[l, tt], wot[l, :, cols])
        return total.astype(jnp.bfloat16)

    mine = pl.ds(pl.multiple_of(x * rows, rows), rows)
    for l in range(2):
        if l == 0:
            sent, send = gather_start(0, lambda h: tok.at[pl.ds(h * half, half)])
            xg[0, t, mine, :] = tok[...]
            shared = []
            for ll in range(2):
                for q in range(6):
                    copy = remote(
                        weights[q].at[ll], wcat.at[ll, wrow(q)],
                        wc_send.at[ll, q], wc_recv.at[ll, q], t, sibling,
                    )
                    copy.start()
                    shared.append(copy)
        else:
            xg[1, t, mine, :] = current
            sent, send = gather_start(1, lambda h: xg.at[1, t, own_rows(h, x)])
        gather_relay(l, send)
        if l == 0:
            prepare(0)
        traded = project(l)
        folded = out_start(l)
        for copy in sent:
            copy.wait_send()
        mixed = recur(l)
        out_relay(l, folded)
        if l == 0:
            prepare(1)
        out_finish(l, folded)
        current = fold(l)
        for copy in traded + folded + mixed:
            copy.wait_send()
    mixed_ref[...] = current
    for copy in shared:
        copy.wait_send()


def step(tok, lens, gain, base, rate, ggain, weights, wo, state, tp, dp):
    rows, width = tok.shape
    slim = width // dp
    nx = dp // 2
    feat = tp * width
    bf = jnp.bfloat16
    vmem, any_ = pl.BlockSpec(memory_space=pltpu.VMEM), pl.BlockSpec(memory_space=pl.ANY)
    dma = pltpu.SemaphoreType.DMA
    half = rows // 2
    return pl.pallas_call(
        functools.partial(step_body, tp=tp, dp=dp),
        out_shape=(
            jax.ShapeDtypeStruct((rows, width), bf),
            jax.ShapeDtypeStruct((2, 4, nx, rows, 2 * slim), jnp.float32),
        ),
        in_specs=[vmem] * 6 + [any_] * 8,
        out_specs=(vmem, vmem),
        scratch_shapes=[
            pltpu.VMEM((2, tp, nx * rows, width), bf),
            pltpu.VMEM((2, 12 * slim, feat), bf),
            pltpu.VMEM((2, width, feat), bf),
            pltpu.VMEM((2, nx, rows, 12 * slim), bf),
            pltpu.VMEM((2, tp, rows, width), bf),
            pltpu.VMEM((2, nx, rows, 12 * slim), bf),
            pltpu.VMEM(state.shape, state.dtype),
            pltpu.VMEM((nx * rows, 12 * slim), jnp.float32),
            pltpu.VMEM((nx * rows, 128), jnp.float32),
            dma(((nx - 1) * (tp + 1) + (tp - 1) * (nx + 1),)),
            dma((2, nx)),
            dma((2, tp)),
            dma((2, tp)),
            dma((2, nx)),
            dma((2, nx)),
            dma((2, 2 * tp)),
            dma((2, tp)),
            dma((2, 8)),
            dma((2, 8)),
            dma((2, 6)),
            dma((2, 6)),
            dma((2, 7)),
            dma((2,)),
        ],
        compiler_params=pltpu.CompilerParams(
            collective_id=0, has_side_effects=True, vmem_limit_bytes=VMEM_LIMIT
        ),
        name="step",
    )(tok, lens, gain, base, rate, ggain, *weights, wo, state)


def renew_body(rows_ref, mixed_ref, state_ref, new_ref, out_ref):
    group, heads, size = state_ref.shape[1:4]
    across = lax.broadcasted_iota(jnp.int32, (size, size), 0)
    along = lax.broadcasted_iota(jnp.int32, (size, size), 1)
    eye = across == along

    @pl.when((pl.program_id(0) == 0) & (pl.program_id(1) == 0))
    def _():
        out_ref[...] = mixed_ref[...]

    for b in range(group):
        for h in range(heads):
            neg, held, decay, rated = [rows_ref[0, q, h, b : b + 1, :] for q in range(4)]
            old = state_ref[0, b, h]
            weight = jnp.sum(old * neg + jnp.where(eye, held, 0.0), axis=1, keepdims=True)
            new_ref[0, b, h] = old * decay + weight * rated


def renew(rows, mixed, state):
    group = 8
    heads, size = state.shape[2:4]
    block = pl.BlockSpec((1, group, heads, size, size), lambda l, i: (l, i, 0, 0, 0))
    whole = pl.BlockSpec(mixed.shape, lambda l, i: (0, 0))
    return pl.pallas_call(
        renew_body,
        grid=(2, state.shape[1] // group),
        out_shape=(
            jax.ShapeDtypeStruct(state.shape, state.dtype),
            jax.ShapeDtypeStruct(mixed.shape, mixed.dtype),
        ),
        in_specs=[
            pl.BlockSpec((1, 4, heads, group, size), lambda l, i: (l, 0, 0, i, 0)),
            whole,
            block,
        ],
        out_specs=(block, whole),
        compiler_params=pltpu.CompilerParams(vmem_limit_bytes=VMEM_LIMIT),
        name="renew",
    )(rows, mixed, state)


def on_device(
    tokens,
    lengths,
    norm_gain,
    w_recept,
    w_key,
    w_value,
    w_decay,
    w_rate,
    w_gate,
    w_out,
    decay_base,
    rate_base,
    group_gain,
    state,
):
    tp, dp = lax.axis_size("tp"), lax.axis_size("dp")
    weights = [w.transpose(0, 2, 1) for w in (w_recept, w_key, w_value, w_decay, w_rate, w_gate)]
    mixed, rows = step(
        tokens, lengths.reshape(1, -1), norm_gain, decay_base, rate_base, group_gain,
        weights, w_out.transpose(0, 2, 1), state, tp, dp,
    )
    states, mixed = renew(rows, mixed, state)
    return (mixed, states)


def solution(mesh):
    columns = P(None, None, ("tp", "dp"))
    in_specs = (
        (P("dp", "tp"), P("dp"), P())
        + (columns,) * 7
        + (P(None, "tp"),) * 3
        + (P(None, "dp", "tp", None, None),)
    )
    out_specs = (P("dp", "tp"), P(None, "dp", "tp", None, None))
    return jax.shard_map(
        on_device, mesh=mesh, in_specs=in_specs, out_specs=out_specs, check_vma=False
    )
```

time: 280 us -> 79.1 us (0.28)
  the two profiles are of different devices: /device:TPU:0 before, /device:TPU:1 now
where the time goes in v1:
time: 79.1 us; the launch traced here: 78.7 us
  Pallas kernels  78 us (99%)
    pallas_call x1, Pallas kernels, step(): pl.pallas_call(functools.partial(step_body, tp=tp, dp=dp), out_shape=(jax...  67.9 us
    pallas_call x1, Pallas kernels, renew(): pl.pallas_call(renew_body, grid=(2, state.shape[1] // group), out_shape=(...  10.2 us

profile of v1, /device:TPU:1, one launch (start us, length us, event | category | flops | bytes accessed | tf_op | source)
XLA Modules:
  0.0 78.7 jit_solution(1117269032945846032)
XLA Ops:
  0.6 67.9 %step.1 = (bf16[32,256]{1,0:T(8,128)(2,1)}, f32[2,4,4,32,64]{4,3,2,1,0:T(8,128)}) custom-call(bf16[32,256]{1,0:T(8,128)(2,1)} %tok.1, s32[1,32]{1,0:T(1,128)} %bitcast.15, f32[2,4096]{1,0:T(2,128)} %gain.1, f32[2,256]{1,0:T(2,128)} %base.1, f32[2,256]{1,0:T(2,128)} %rate.1, f32[2,256]{1,0:T(2,128)} %ggain.1, bf16[2,32,4096]{2,1,0:T(8,128)(2,1)} %bitcast.8, ...), custom_call_target="tpu_custom_call" | custom-call | tf_op jit(solution)/shard_map/step/pallas_call | solution.py:332
  68.5 10.2 %renew.1 = (f32[2,32,4,64,64]{4,3,2,1,0:T(8,128)}, bf16[32,256]{1,0:T(8,128)(2,1)}) custom-call(f32[2,4,4,32,64]{4,3,2,1,0:T(8,128)} %get-tuple-element.6.rows_ref, bf16[32,256]{1,0:T(8,128)(2,1)} %get-tuple-element.7.mixed_ref, f32[2,32,4,64,64]{4,3,2,1,0:T(8,128)} %state_ref.1), custom_call_target="tpu_custom_call" | custom-call | tf_op jit(solution)/shard_map/renew/pallas_call | solution.py:395

commit v2 on v1

--- a/solution.py
+++ b/solution.py
@@ -1,3 +1,4 @@
+import contextlib
 import functools
 
 import jax
@@ -10,8 +11,12 @@
 STEP = 16
 RMS_EPS = 1e-06
 GROUP_EPS = 0.00064
-VMEM_LIMIT = 56 * 1024 * 1024
+VMEM_LIMIT = 55_000_000
 MESH = pl.DeviceIdType.MESH
+
+
+def scope(name):
+    return contextlib.nullcontext()
 
 
 def dot_t(a, b):
@@ -28,11 +33,12 @@
 
 
 def step_body(
-    tok, lens, gain, base, rate, ggain, wr, wk, wv, wd, wa, wg, wo, state,
-    mixed_ref, rows_ref,
-    xg, wcat, wot, vg, mg, pieces, st, acc, square,
+    tok, lens_hbm, gain_hbm, base_hbm, rate_hbm, ggain_hbm, wr, wk, wv, wd, wa, wg, wo, state,
+    mixed_ref, st,
+    xg, wcat, wot, vg, mg, pieces, turned, rows_ref, acc, square,
+    lens, gain, base, rate, ggain,
     ag_send, a1_recv, b1_recv, fin_recv, ex_send, ex_recv, mg_send, mg_recv,
-    wo_send, wo_recv, wc_send, wc_recv, own_sem, st_sem,
+    wo_send, wo_recv, wc_send, wc_recv, own_sem, st_sem, small_sem,
     *, tp, dp,
 ):
     t, d = lax.axis_index("tp"), lax.axis_index("dp")
@@ -80,15 +86,44 @@
     def worow(dd, start=0, count=None):
         return pl.ds(pl.multiple_of(dd * slim + start, slim // 2), slim if count is None else count)
 
+    mine = pl.ds(pl.multiple_of(x * rows, rows), rows)
+    own_tok = fetch(tok, xg.at[0, t, mine], small_sem.at[5])
+    small = [
+        fetch(src, dst, small_sem.at[i])
+        for i, (src, dst) in enumerate(
+            [(lens_hbm, lens), (gain_hbm, gain), (base_hbm, base), (rate_hbm, rate), (ggain_hbm, ggain)]
+        )
+    ]
+    own_s = [fetch(state.at[0], st.at[0], st_sem.at[0])]
     own_w = [[fetch(weights[q].at[l], wcat.at[l, wrow(q)], own_sem.at[l, q]) for q in range(6)] for l in range(2)]
     own_o = [fetch(wo.at[l], wot.at[l, worow(d)], own_sem.at[l, 6]) for l in range(2)]
-    own_s = [fetch(state.at[l], st.at[l], st_sem.at[l]) for l in range(2)]
+    own_s.append(fetch(state.at[1], st.at[1], st_sem.at[1]))
 
     barrier = pltpu.get_barrier_semaphore()
     everyone = [(p, d) for p in far] + [(t, 2 * o + core) for o in xs] + [(t, sibling)]
     for p in everyone:
         pl.semaphore_signal(barrier, inc=1, device_id=p, device_id_type=MESH)
-    pl.semaphore_wait(barrier, len(everyone))
+
+    def turn(l):
+        own_s[l].wait()
+
+        def one(i, carry):
+            for k in range(4):
+                for p in range(nx // 2):
+                    both = jnp.concatenate([st[l, i * 4 + k, 2 * p], st[l, i * 4 + k, 2 * p + 1]], axis=0)
+                    turned[l, i * 4 + k, :, p * 128 : (p + 1) * 128] = both.T.astype(jnp.bfloat16)
+            return carry
+
+        lax.fori_loop(0, rows // 4, one, 0)
+
+    with scope("turn0"):
+        turn(0)
+    with scope("barrier"):
+        pl.semaphore_wait(barrier, len(everyone))
+    with scope("small"):
+        for copy in small:
+            copy.wait()
+        own_tok.wait()
 
     def own_rows(h, xx):
         return pl.ds(pl.multiple_of(xx * rows + h * half, half), half)
@@ -113,16 +148,18 @@
         return sent, send
 
     def gather_relay(l, send):
-        for o in xs:
-            block = xg.at[l, t, own_rows(0, o)]
-            arrived(block, a1_recv.at[l, o])
-            for p in far:
-                send(block, block, fin_recv.at[l, t], p, d)
-        for p in peers:
-            block = xg.at[l, p, own_rows(1, x)]
-            arrived(block, b1_recv.at[l, p])
-            for o in xs:
-                send(block, block, fin_recv.at[l, p], t, 2 * o + core)
+        for i, o in enumerate(xs):
+            with scope(f"a{l}_{i}"):
+                block = xg.at[l, t, own_rows(0, o)]
+                arrived(block, a1_recv.at[l, o])
+                for p in far:
+                    send(block, block, fin_recv.at[l, t], p, d)
+        for i, p in enumerate(peers):
+            with scope(f"b{l}_{i}"):
+                block = xg.at[l, p, own_rows(1, x)]
+                arrived(block, b1_recv.at[l, p])
+                for o in xs:
+                    send(block, block, fin_recv.at[l, p], t, 2 * o + core)
 
     def prepare(l):
         for q in range(6):
@@ -145,7 +182,8 @@
         for o in offs:
             tt = plane(o)
             count = (nx - 1) * half if o == (0, 0) else (2 * nx - 1) * half
-            arrived(xg.at[l, tt, pl.ds(0, count)], fin_recv.at[l, tt])
+            with scope(f"x{l}_{o[0]}_{o[1]}"):
+                arrived(xg.at[l, tt, pl.ds(0, count)], fin_recv.at[l, tt])
             block = xg[l, tt]
             cols = pl.ds(pl.multiple_of(tt * width, width), width)
             acc[...] += dot_t(block, wcat[l, :, cols])
@@ -218,12 +256,22 @@
     lane = lax.broadcasted_iota(jnp.int32, (rows, rows), 1)
     spread = jnp.where(sub == lane, lens[...].astype(jnp.float32), 0.0)
     live = jnp.sum(spread, axis=1, keepdims=True) > STEP
-    eight = lax.broadcasted_iota(jnp.int32, (8, size), 0)
+    eight = lax.broadcasted_iota(jnp.int32, (8, 2 * size), 0)
+    left = lax.broadcasted_iota(jnp.int32, (8, 2 * size), 1) < size
+    left_half = lax.broadcasted_iota(jnp.int32, (half, 2 * size), 1) < size
+
+    def paired(parts, p):
+        return jnp.concatenate([parts[2 * p], parts[2 * p + 1]], axis=1)
+
+    def by_head(values):
+        one = jnp.sum(jnp.where(left_half, values, 0.0), axis=1, keepdims=True)
+        two = jnp.sum(jnp.where(left_half, 0.0, values), axis=1, keepdims=True)
+        return jnp.where(left_half, one, two) / size
 
     def recur(l):
-        for o in xs:
-            arrived(vg.at[l, o], ex_recv.at[l, o])
-        own_s[l].wait()
+        with scope(f"exchange{l}"):
+            for o in xs:
+                arrived(vg.at[l, o], ex_recv.at[l, o])
         looks, extras, gates = [], [], []
         for h in range(nx):
             part = slice(h * size, (h + 1) * size)
@@ -233,36 +281,40 @@
             decay = jnp.exp(-jnp.exp(-jax.nn.softplus(-(base[l : l + 1, part] + decay_pre)) - 0.5))
             learn = jax.nn.sigmoid(rate[l : l + 1, part] + rate_pre)
             length = jnp.maximum(jnp.sqrt(jnp.sum(key * key, axis=1, keepdims=True)), 1e-12)
+            blend = jnp.sum(key * learn * recept, axis=1, keepdims=True)
             unit = key / length
-            rated = unit * learn
             held = value * length
-            rho = jnp.sum(rated * recept, axis=1, keepdims=True)
             rows_ref[l, 0, h] = jnp.where(live, -unit, 0.0)
             rows_ref[l, 1, h] = jnp.where(live, held, 0.0)
             rows_ref[l, 2, h] = jnp.where(live, decay, 1.0)
-            rows_ref[l, 3, h] = rated
-            looks.append(decay * recept - rho * unit)
-            extras.append(rho * held)
+            rows_ref[l, 3, h] = unit * learn
+            looks.append(decay * recept - (blend / length) * unit)
+            extras.append(blend * value)
             gates.append(jax.nn.sigmoid(gate_pre) * ggain[l : l + 1, part])
+        gates = [paired(gates, p) for p in range(nx // 2)]
+        extras = [paired(extras, p) for p in range(nx // 2)]
         sent = []
         for g in range(2):
+            reads = [[] for p in range(nx // 2)]
+            for k in range(half // 8):
+                low = g * half + k * 8
+                look = jnp.concatenate([v[low : low + 8] for v in looks], axis=0).astype(jnp.bfloat16)
+                sums = [extras[p][low : low + 8] for p in range(nx // 2)]
+                for b in range(8):
+                    got = jnp.dot(look, turned[l, low + b], preferred_element_type=jnp.float32)
+                    for h in range(nx):
+                        p = h // 2
+                        side = left if h % 2 == 0 else jnp.logical_not(left)
+                        piece = got[h * 8 : (h + 1) * 8, p * 128 : (p + 1) * 128]
+                        sums[p] += jnp.where((eight == b) & side, piece, 0.0)
+                for p in range(nx // 2):
+                    reads[p].append(sums[p])
+            span = slice(g * half, (g + 1) * half)
             outs = []
-            for h in range(nx):
-                reads = []
-                for k in range(half // 8):
-                    low = g * half + k * 8
-                    look = looks[h][low : low + 8]
-                    read = extras[h][low : low + 8]
-                    for b in range(8):
-                        got = dot_t(look, st[l, low + b, h])
-                        read += jnp.where(eight == b, got, 0.0)
-                    reads.append(read)
-                read = jnp.concatenate(reads, axis=0)
-                span = slice(g * half, (g + 1) * half)
-                centre = jnp.mean(read, axis=1, keepdims=True)
-                apart = read - centre
-                var = jnp.mean(apart * apart, axis=1, keepdims=True)
-                normal = apart * lax.rsqrt(var + GROUP_EPS) * gates[h][span]
+            for p in range(nx // 2):
+                read = jnp.concatenate(reads[p], axis=0)
+                apart = read - by_head(read)
+                normal = apart * lax.rsqrt(by_head(apart * apart) + GROUP_EPS) * gates[p][span]
                 outs.append(jnp.where(live[span], normal, 0.0).astype(jnp.bfloat16))
             span = pl.ds(g * half, half)
             mg[l, t, span, :] = jnp.concatenate(outs, axis=1)
@@ -273,46 +325,74 @@
                 sent.append(copy)
         return sent
 
+    eye = lax.broadcasted_iota(jnp.int32, (size, size), 0) == lax.broadcasted_iota(jnp.int32, (size, size), 1)
+
+    def update(l):
+        def one(i, carry):
+            for k in range(4):
+                b = i * 4 + k
+                for h in range(nx):
+                    neg, held, decay, rated = [rows_ref[l, q, h, pl.ds(b, 1), :] for q in range(4)]
+                    old = st[l, b, h]
+                    weight = jnp.sum(old * neg + jnp.where(eye, held, 0.0), axis=1, keepdims=True)
+                    st[l, b, h] = old * decay + weight * rated
+            return carry
+
+        lax.fori_loop(0, rows // 4, one, 0)
+
     def fold(l):
         total = jnp.zeros((rows, width), jnp.float32)
         for o in offs:
             tt = plane(o)
             if o != (0, 0):
-                arrived(mg.at[l, tt], mg_recv.at[l, tt])
+                with scope(f"m{l}_{o[0]}_{o[1]}"):
+                    arrived(mg.at[l, tt], mg_recv.at[l, tt])
             cols = pl.ds(pl.multiple_of(tt * width, width), width)
             total += dot_t(mg[l, tt], wot[l, :, cols])
         return total.astype(jnp.bfloat16)
 
-    mine = pl.ds(pl.multiple_of(x * rows, rows), rows)
     for l in range(2):
-        if l == 0:
-            sent, send = gather_start(0, lambda h: tok.at[pl.ds(h * half, half)])
-            xg[0, t, mine, :] = tok[...]
-            shared = []
-            for ll in range(2):
-                for q in range(6):
-                    copy = remote(
-                        weights[q].at[ll], wcat.at[ll, wrow(q)],
-                        wc_send.at[ll, q], wc_recv.at[ll, q], t, sibling,
-                    )
-                    copy.start()
-                    shared.append(copy)
-        else:
-            xg[1, t, mine, :] = current
-            sent, send = gather_start(1, lambda h: xg.at[1, t, own_rows(h, x)])
+        with scope(f"start{l}"):
+            if l == 1:
+                xg[1, t, mine, :] = current
+            sent, send = gather_start(l, lambda h: xg.at[l, t, own_rows(h, x)])
+            if l == 0:
+                shared = []
+                for ll in range(2):
+                    for q in range(6):
+                        copy = remote(
+                            weights[q].at[ll], wcat.at[ll, wrow(q)],
+                            wc_send.at[ll, q], wc_recv.at[ll, q], t, sibling,
+                        )
+                        copy.start()
+                        shared.append(copy)
         gather_relay(l, send)
         if l == 0:
-            prepare(0)
-        traded = project(l)
-        folded = out_start(l)
-        for copy in sent:
-            copy.wait_send()
-        mixed = recur(l)
-        out_relay(l, folded)
+            with scope("prepare0"):
+                prepare(0)
+        else:
+            with scope("update0"):
+                update(0)
+        with scope(f"project{l}"):
+            traded = project(l)
+            folded = out_start(l)
+            for copy in sent:
+                copy.wait_send()
+        with scope(f"recur{l}"):
+            mixed = recur(l)
+        with scope(f"outrelay{l}"):
+            out_relay(l, folded)
         if l == 0:
-            prepare(1)
-        out_finish(l, folded)
-        current = fold(l)
+            with scope("prepare1"):
+                prepare(1)
+                turn(1)
+        else:
+            with scope("update1"):
+                update(1)
+        with scope(f"outfinish{l}"):
+            out_finish(l, folded)
+        with scope(f"fold{l}"):
+            current = fold(l)
         for copy in traded + folded + mixed:
             copy.wait_send()
     mixed_ref[...] = current
@@ -326,16 +406,16 @@
     nx = dp // 2
     feat = tp * width
     bf = jnp.bfloat16
-    vmem, any_ = pl.BlockSpec(memory_space=pltpu.VMEM), pl.BlockSpec(memory_space=pl.ANY)
+    vmem, hbm = pl.BlockSpec(memory_space=pltpu.VMEM), pl.BlockSpec(memory_space=pltpu.HBM)
     dma = pltpu.SemaphoreType.DMA
     half = rows // 2
     return pl.pallas_call(
         functools.partial(step_body, tp=tp, dp=dp),
         out_shape=(
-            jax.ShapeDtypeStruct((rows, width), bf),
-            jax.ShapeDtypeStruct((2, 4, nx, rows, 2 * slim), jnp.float32),
+            pltpu.VMEM((rows, width), bf),
+            pltpu.VMEM(state.shape, state.dtype),
         ),
-        in_specs=[vmem] * 6 + [any_] * 8,
+        in_specs=[hbm] * 14,
         out_specs=(vmem, vmem),
         scratch_shapes=[
             pltpu.VMEM((2, tp, nx * rows, width), bf),
@@ -344,9 +424,15 @@
             pltpu.VMEM((2, nx, rows, 12 * slim), bf),
             pltpu.VMEM((2, tp, rows, width), bf),
             pltpu.VMEM((2, nx, rows, 12 * slim), bf),
-            pltpu.VMEM(state.shape, state.dtype),
+            pltpu.VMEM((2, rows, 2 * slim, nx * 2 * slim), bf),
+            pltpu.VMEM((2, 4, nx, rows, 2 * slim), jnp.float32),
             pltpu.VMEM((nx * rows, 12 * slim), jnp.float32),
             pltpu.VMEM((nx * rows, 128), jnp.float32),
+            pltpu.VMEM(lens.shape, lens.dtype),
+            pltpu.VMEM(gain.shape, gain.dtype),
+            pltpu.VMEM(base.shape, base.dtype),
+            pltpu.VMEM(rate.shape, rate.dtype),
+            pltpu.VMEM(ggain.shape, ggain.dtype),
             dma(((nx - 1) * (tp + 1) + (tp - 1) * (nx + 1),)),
             dma((2, nx)),
             dma((2, tp)),
@@ -361,6 +447,7 @@
             dma((2, 6)),
             dma((2, 7)),
             dma((2,)),
+            dma((6,)),
         ],
         compiler_params=pltpu.CompilerParams(
             collective_id=0, has_side_effects=True, vmem_limit_bytes=VMEM_LIMIT
@@ -369,45 +456,35 @@
     )(tok, lens, gain, base, rate, ggain, *weights, wo, state)
 
 
-def renew_body(rows_ref, mixed_ref, state_ref, new_ref, out_ref):
-    group, heads, size = state_ref.shape[1:4]
-    across = lax.broadcasted_iota(jnp.int32, (size, size), 0)
-    along = lax.broadcasted_iota(jnp.int32, (size, size), 1)
-    eye = across == along
-
-    @pl.when((pl.program_id(0) == 0) & (pl.program_id(1) == 0))
-    def _():
-        out_ref[...] = mixed_ref[...]
-
-    for b in range(group):
-        for h in range(heads):
-            neg, held, decay, rated = [rows_ref[0, q, h, b : b + 1, :] for q in range(4)]
-            old = state_ref[0, b, h]
-            weight = jnp.sum(old * neg + jnp.where(eye, held, 0.0), axis=1, keepdims=True)
-            new_ref[0, b, h] = old * decay + weight * rated
-
-
-def renew(rows, mixed, state):
-    group = 8
-    heads, size = state.shape[2:4]
-    block = pl.BlockSpec((1, group, heads, size, size), lambda l, i: (l, i, 0, 0, 0))
-    whole = pl.BlockSpec(mixed.shape, lambda l, i: (0, 0))
+def put_body(mixed_ref, state_ref, out_ref, new_ref, sem):
+    count = state_ref.shape[0] * 4
+    part = state_ref.shape[1] // 4
+    copies = [pltpu.make_async_copy(mixed_ref, out_ref, sem.at[count])]
+    for i in range(count):
+        span = pl.ds(i % 4 * part, part)
+        copies.append(
+            pltpu.make_async_copy(state_ref.at[i // 4, span], new_ref.at[i // 4, span], sem.at[i])
+        )
+    for copy in copies:
+        copy.start()
+    for copy in copies:
+        copy.wait()
+
+
+def put(mixed, state):
+    vmem, hbm = pl.BlockSpec(memory_space=pltpu.VMEM), pl.BlockSpec(memory_space=pltpu.HBM)
     return pl.pallas_call(
-        renew_body,
-        grid=(2, state.shape[1] // group),
+        put_body,
         out_shape=(
+            jax.ShapeDtypeStruct(mixed.shape, mixed.dtype),
             jax.ShapeDtypeStruct(state.shape, state.dtype),
-            jax.ShapeDtypeStruct(mixed.shape, mixed.dtype),
         ),
-        in_specs=[
-            pl.BlockSpec((1, 4, heads, group, size), lambda l, i: (l, 0, 0, i, 0)),
-            whole,
-            block,
-        ],
-        out_specs=(block, whole),
-        compiler_params=pltpu.CompilerParams(vmem_limit_bytes=VMEM_LIMIT),
-        name="renew",
-    )(rows, mixed, state)
+        in_specs=[vmem, vmem],
+        out_specs=(hbm, hbm),
+        scratch_shapes=[pltpu.SemaphoreType.DMA((state.shape[0] * 4 + 1,))],
+        compiler_params=pltpu.CompilerParams(vmem_limit_bytes=4 * 1024 * 1024),
+        name="put",
+    )(mixed, state)
 
 
 def on_device(
@@ -428,12 +505,11 @@
 ):
     tp, dp = lax.axis_size("tp"), lax.axis_size("dp")
     weights = [w.transpose(0, 2, 1) for w in (w_recept, w_key, w_value, w_decay, w_rate, w_gate)]
-    mixed, rows = step(
+    mixed, states = step(
         tokens, lengths.reshape(1, -1), norm_gain, decay_base, rate_base, group_gain,
         weights, w_out.transpose(0, 2, 1), state, tp, dp,
     )
-    states, mixed = renew(rows, mixed, state)
-    return (mixed, states)
+    return put(mixed, states)
 
 
 def solution(mesh):

time: 79.1 us -> 71.5 us (0.904)
  Pallas kernels: 78 us -> 70.8 us
    pallas_call x2, Pallas kernels: 78 us -> 70.8 us  [the longest x1 67.4 us: step(): pl.pallas_call(functools.partial(step_body, tp=tp, dp=dp), out_shape=(plt...]
where the time goes in v2:
time: 71.5 us; the launch traced here: 71.4 us
  Pallas kernels  70.8 us (99%)
    pallas_call x1, Pallas kernels, step(): pl.pallas_call(functools.partial(step_body, tp=tp, dp=dp), out_shape=(plt...  67.4 us
    pallas_call x1, Pallas kernels, put(): pl.pallas_call(put_body, out_shape=(jax.ShapeDtypeStruct(mixed.shape, mix...  3.38 us

profile of v2, /device:TPU:1, one launch (start us, length us, event | category | flops | bytes accessed | tf_op | source)
XLA Modules:
  0.0 71.4 jit_solution(11679580512236815821)
XLA Ops:
  0.6 67.4 %step.1 = (bf16[32,256]{1,0:T(8,128)(2,1)S(1)}, f32[2,32,4,64,64]{4,3,2,1,0:T(8,128)S(1)}) custom-call(bf16[32,256]{1,0:T(8,128)(2,1)} %tok.1, s32[1,32]{1,0:T(1,128)} %bitcast.15, f32[2,4096]{1,0:T(2,128)} %gain_hbm.1, f32[2,256]{1,0:T(2,128)} %base_hbm.1, f32[2,256]{1,0:T(2,128)} %rate_hbm.1, f32[2,256]{1,0:T(2,128)} %ggain_hbm.1, ...), custom_call_target="tpu_custom_call" | custom-call | tf_op jit(solution)/shard_map/step/pallas_call | solution.py:412
  68.0 3.4 %put.1 = (bf16[32,256]{1,0:T(8,128)(2,1)}, f32[2,32,4,64,64]{4,3,2,1,0:T(8,128)}) custom-call(bf16[32,256]{1,0:T(8,128)(2,1)S(1)} %get-tuple-element.4.mixed_ref, f32[2,32,4,64,64]{4,3,2,1,0:T(8,128)S(1)} %get-tuple-element.5.state_ref), custom_call_target="tpu_custom_call" | custom-call | tf_op jit(solution)/shard_map/put/pallas_call | solution.py:476

commit v3 on v2

--- a/solution.py
+++ b/solution.py
@@ -73,7 +73,6 @@
     ks = [1, nx - 1] + list(range(2, nx - 1))
     xs = [xpeer(k) for k in ks]
 
-    local = []
 
     def fetch(src, dst, sem):
         copy = pltpu.make_async_copy(src, dst, sem)
@@ -88,6 +87,10 @@
 
     mine = pl.ds(pl.multiple_of(x * rows, rows), rows)
     own_tok = fetch(tok, xg.at[0, t, mine], small_sem.at[5])
+    barrier = pltpu.get_barrier_semaphore()
+    everyone = [(p, d) for p in far] + [(t, 2 * o + core) for o in xs] + [(t, sibling)]
+    for p in everyone:
+        pl.semaphore_signal(barrier, inc=1, device_id=p, device_id_type=MESH)
     small = [
         fetch(src, dst, small_sem.at[i])
         for i, (src, dst) in enumerate(
@@ -99,10 +102,6 @@
     own_o = [fetch(wo.at[l], wot.at[l, worow(d)], own_sem.at[l, 6]) for l in range(2)]
     own_s.append(fetch(state.at[1], st.at[1], st_sem.at[1]))
 
-    barrier = pltpu.get_barrier_semaphore()
-    everyone = [(p, d) for p in far] + [(t, 2 * o + core) for o in xs] + [(t, sibling)]
-    for p in everyone:
-        pl.semaphore_signal(barrier, inc=1, device_id=p, device_id_type=MESH)
 
     def turn(l):
         own_s[l].wait()
@@ -116,8 +115,6 @@
 
         lax.fori_loop(0, rows // 4, one, 0)
 
-    with scope("turn0"):
-        turn(0)
     with scope("barrier"):
         pl.semaphore_wait(barrier, len(everyone))
     with scope("small"):
@@ -148,18 +145,20 @@
         return sent, send
 
     def gather_relay(l, send):
-        for i, o in enumerate(xs):
-            with scope(f"a{l}_{i}"):
-                block = xg.at[l, t, own_rows(0, o)]
-                arrived(block, a1_recv.at[l, o])
-                for p in far:
-                    send(block, block, fin_recv.at[l, t], p, d)
-        for i, p in enumerate(peers):
-            with scope(f"b{l}_{i}"):
-                block = xg.at[l, p, own_rows(1, x)]
-                arrived(block, b1_recv.at[l, p])
-                for o in xs:
-                    send(block, block, fin_recv.at[l, p], t, 2 * o + core)
+        steps = [("a", o) for o in xs[:2]] + [("b", p) for p in peers[:4]]
+        steps += [("a", o) for o in xs[2:]] + [("b", p) for p in peers[4:]]
+        for i, (kind, o) in enumerate(steps):
+            with scope(f"{kind}{l}_{i}"):
+                if kind == "a":
+                    block = xg.at[l, t, own_rows(0, o)]
+                    arrived(block, a1_recv.at[l, o])
+                    for p in far:
+                        send(block, block, fin_recv.at[l, t], p, d)
+                else:
+                    block = xg.at[l, o, own_rows(1, x)]
+                    arrived(block, b1_recv.at[l, o])
+                    for p in xs:
+                        send(block, block, fin_recv.at[l, o], t, 2 * p + core)
 
     def prepare(l):
         for q in range(6):
@@ -205,51 +204,54 @@
         vg[l, x] = pieces[l, x]
         return sent
 
-    def out_slot(l, xx, cc, start=0, count=None):
+    part = slim // 2
+    up, down, across = xpeer(1), xpeer(-1), xpeer(2)
+
+    def out_piece(l, xx, cc, piece):
+        start, count = (0, slim) if piece is None else (piece * part, part)
         return wot.at[l, worow(2 * xx + cc, start, count)]
 
-    def out_start(l):
-        own_o[l].wait()
-        up, down = xpeer(1), xpeer(-1)
-        block = out_slot(l, x, core)
-        sent = [
-            remote(block, block, wo_send.at[l, 0], wo_recv.at[l, 0], t, 2 * up + core),
-            remote(block, block, wo_send.at[l, 1], wo_recv.at[l, 1], t, 2 * down + core),
-            remote(block, block, wo_send.at[l, 2], wo_recv.at[l, 4], t, sibling),
-        ]
-        for copy in sent:
-            copy.start()
-        return sent
-
-    def out_relay(l, sent):
-        up, down, across = xpeer(1), xpeer(-1), xpeer(2)
-        part = slim // 2
-        below, above = out_slot(l, down, core), out_slot(l, up, core)
-        arrived(below, wo_recv.at[l, 0])
-        first = out_slot(l, down, core, 0, part)
-        one = remote(first, first, wo_send.at[l, 3], wo_recv.at[l, 2], t, 2 * up + core)
-        one.start()
-        two = remote(below, below, wo_send.at[l, 4], wo_recv.at[l, 5], t, sibling)
-        two.start()
-        arrived(above, wo_recv.at[l, 1])
-        second = out_slot(l, up, core, part, part)
-        three = remote(second, second, wo_send.at[l, 5], wo_recv.at[l, 3], t, 2 * down + core)
-        three.start()
-        four = remote(above, above, wo_send.at[l, 6], wo_recv.at[l, 6], t, sibling)
-        four.start()
-        sent += [one, two, three, four]
-
-    def out_finish(l, sent):
-        up, down, across = xpeer(1), xpeer(-1), xpeer(2)
-        part = slim // 2
-        arrived(out_slot(l, across, core, 0, part), wo_recv.at[l, 2])
-        arrived(out_slot(l, across, core, part, part), wo_recv.at[l, 3])
-        block = out_slot(l, across, core)
-        copy = remote(block, block, wo_send.at[l, 7], wo_recv.at[l, 7], t, sibling)
+    def out_send(l, sent, n, xx, piece, to_x, to_core):
+        block = out_piece(l, xx, core, piece)
+        copy = remote(block, block, wo_send.at[l, n], wo_recv.at[l, n], t, 2 * to_x + to_core)
         copy.start()
         sent.append(copy)
-        for i, xx in enumerate((x, down, up, across)):
-            arrived(out_slot(l, xx, 1 - core), wo_recv.at[l, 4 + i])
+
+    def out_arrived(l, n, xx, piece, cc=None):
+        arrived(out_piece(l, xx, core if cc is None else cc, piece), wo_recv.at[l, n])
+
+    def out_first(l):
+        own_o[l].wait()
+        sent = []
+        out_send(l, sent, 0, x, 0, up, core)
+        out_send(l, sent, 1, x, 1, down, core)
+        out_send(l, sent, 6, x, None, x, 1 - core)
+        return sent
+
+    def out_second(l, sent):
+        out_arrived(l, 0, down, 0)
+        out_send(l, sent, 4, down, 0, up, core)
+        out_send(l, sent, 7, down, 0, x, 1 - core)
+        out_arrived(l, 1, up, 1)
+        out_send(l, sent, 5, up, 1, down, core)
+        out_send(l, sent, 8, up, 1, x, 1 - core)
+
+    def out_third(l, sent):
+        out_send(l, sent, 2, x, 1, up, core)
+        out_send(l, sent, 3, x, 0, down, core)
+
+    def out_fourth(l, sent):
+        out_arrived(l, 4, across, 0)
+        out_arrived(l, 5, across, 1)
+        out_send(l, sent, 11, across, None, x, 1 - core)
+        out_arrived(l, 2, down, 1)
+        out_send(l, sent, 9, down, 1, x, 1 - core)
+        out_arrived(l, 3, up, 0)
+        out_send(l, sent, 10, up, 0, x, 1 - core)
+
+    def out_finish(l):
+        for n, xx, piece in ((6, x, None), (7, down, 0), (8, up, 1), (9, down, 1), (10, up, 0), (11, across, None)):
+            out_arrived(l, n, xx, piece, 1 - core)
 
     size = 2 * slim
     sub = lax.broadcasted_iota(jnp.int32, (rows, rows), 0)
@@ -366,7 +368,13 @@
                         )
                         copy.start()
                         shared.append(copy)
+            folded = out_first(l)
+        if l == 0:
+            with scope("turn0"):
+                turn(0)
         gather_relay(l, send)
+        with scope(f"outsecond{l}"):
+            out_second(l, folded)
         if l == 0:
             with scope("prepare0"):
                 prepare(0)
@@ -375,13 +383,11 @@
                 update(0)
         with scope(f"project{l}"):
             traded = project(l)
-            folded = out_start(l)
+            out_third(l, folded)
             for copy in sent:
                 copy.wait_send()
         with scope(f"recur{l}"):
             mixed = recur(l)
-        with scope(f"outrelay{l}"):
-            out_relay(l, folded)
         if l == 0:
             with scope("prepare1"):
                 prepare(1)
@@ -389,8 +395,10 @@
         else:
             with scope("update1"):
                 update(1)
+        with scope(f"outfourth{l}"):
+            out_fourth(l, folded)
         with scope(f"outfinish{l}"):
-            out_finish(l, folded)
+            out_finish(l)
         with scope(f"fold{l}"):
             current = fold(l)
         for copy in traded + folded + mixed:
@@ -441,8 +449,8 @@
             dma((2, nx)),
             dma((2, 2 * tp)),
             dma((2, tp)),
-            dma((2, 8)),
-            dma((2, 8)),
+            dma((2, 12)),
+            dma((2, 12)),
             dma((2, 6)),
             dma((2, 6)),
             dma((2, 7)),

time: 71.5 us -> 62.8 us (0.88)
  the two profiles are of different devices: /device:TPU:1 before, /device:TPU:0 now
where the time goes in v3:
time: 62.8 us; the launch traced here: 62.5 us
  Pallas kernels  61.9 us (99%)
  between operations  0.64 us (1%)
    pallas_call x1, Pallas kernels, step(): pl.pallas_call(functools.partial(step_body, tp=tp, dp=dp), out_shape=(plt...  58.5 us
    pallas_call x1, Pallas kernels, put(): pl.pallas_call(put_body, out_shape=(jax.ShapeDtypeStruct(mixed.shape, mix...  3.38 us

profile of v3, /device:TPU:0, one launch (start us, length us, event | category | flops | bytes accessed | tf_op | source)
XLA Modules:
  0.0 62.5 jit_solution(9102960453254317589)
XLA Ops:
  0.6 58.5 %step.1 = (bf16[32,256]{1,0:T(8,128)(2,1)S(1)}, f32[2,32,4,64,64]{4,3,2,1,0:T(8,128)S(1)}) custom-call(bf16[32,256]{1,0:T(8,128)(2,1)} %tok.1, s32[1,32]{1,0:T(1,128)} %bitcast.15, f32[2,4096]{1,0:T(2,128)} %gain_hbm.1, f32[2,256]{1,0:T(2,128)} %base_hbm.1, f32[2,256]{1,0:T(2,128)} %rate_hbm.1, f32[2,256]{1,0:T(2,128)} %ggain_hbm.1, ...), custom_call_target="tpu_custom_call" | custom-call | tf_op jit(solution)/shard_map/step/pallas_call | solution.py:420
  59.1 3.4 %put.1 = (bf16[32,256]{1,0:T(8,128)(2,1)}, f32[2,32,4,64,64]{4,3,2,1,0:T(8,128)}) custom-call(bf16[32,256]{1,0:T(8,128)(2,1)S(1)} %get-tuple-element.4.mixed_ref, f32[2,32,4,64,64]{4,3,2,1,0:T(8,128)S(1)} %get-tuple-element.5.state_ref), custom_call_target="tpu_custom_call" | custom-call | tf_op jit(solution)/shard_map/put/pallas_call | solution.py:484

commit v4 on v3

--- a/solution.py
+++ b/solution.py
@@ -241,13 +241,15 @@
         out_send(l, sent, 3, x, 0, down, core)
 
     def out_fourth(l, sent):
-        out_arrived(l, 4, across, 0)
-        out_arrived(l, 5, across, 1)
-        out_send(l, sent, 11, across, None, x, 1 - core)
         out_arrived(l, 2, down, 1)
         out_send(l, sent, 9, down, 1, x, 1 - core)
         out_arrived(l, 3, up, 0)
         out_send(l, sent, 10, up, 0, x, 1 - core)
+
+    def out_fifth(l, sent):
+        out_arrived(l, 4, across, 0)
+        out_arrived(l, 5, across, 1)
+        out_send(l, sent, 11, across, None, x, 1 - core)
 
     def out_finish(l):
         for n, xx, piece in ((6, x, None), (7, down, 0), (8, up, 1), (9, down, 1), (10, up, 0), (11, across, None)):
@@ -271,6 +273,13 @@
         return jnp.where(left_half, one, two) / size
 
     def recur(l):
+        if l == 0:
+            with scope("prepare1"):
+                prepare(1)
+                turn(1)
+        else:
+            with scope("update0"):
+                update(0)
         with scope(f"exchange{l}"):
             for o in xs:
                 arrived(vg.at[l, o], ex_recv.at[l, o])
@@ -368,40 +377,40 @@
                         )
                         copy.start()
                         shared.append(copy)
-            folded = out_first(l)
+            if l == 0:
+                folded = [out_first(0)]
+            else:
+                out_second(1, folded[1])
         if l == 0:
             with scope("turn0"):
                 turn(0)
         gather_relay(l, send)
-        with scope(f"outsecond{l}"):
-            out_second(l, folded)
         if l == 0:
             with scope("prepare0"):
                 prepare(0)
-        else:
-            with scope("update0"):
-                update(0)
         with scope(f"project{l}"):
             traded = project(l)
-            out_third(l, folded)
+            out_third(l, folded[l])
+            if l == 0:
+                out_second(0, folded[0])
             for copy in sent:
                 copy.wait_send()
         with scope(f"recur{l}"):
             mixed = recur(l)
-        if l == 0:
-            with scope("prepare1"):
-                prepare(1)
-                turn(1)
-        else:
+        with scope(f"outfourth{l}"):
+            out_fourth(l, folded[l])
+            if l == 0:
+                folded.append(out_first(1))
+        with scope(f"outfifth{l}"):
+            out_fifth(l, folded[l])
+        if l == 1:
             with scope("update1"):
                 update(1)
-        with scope(f"outfourth{l}"):
-            out_fourth(l, folded)
         with scope(f"outfinish{l}"):
             out_finish(l)
         with scope(f"fold{l}"):
             current = fold(l)
-        for copy in traded + folded + mixed:
+        for copy in traded + folded[l] + mixed:
             copy.wait_send()
     mixed_ref[...] = current
     for copy in shared:

time: 62.8 us -> 62.1 us (0.989)
  no operation moved by 1% of the time
where the time goes in v4:
time: 62.1 us; the launch traced here: 62 us
  Pallas kernels  61.4 us (99%)
  between operations  0.64 us (1%)
    pallas_call x1, Pallas kernels, step(): pl.pallas_call(functools.partial(step_body, tp=tp, dp=dp), out_shape=(plt...  58 us
    pallas_call x1, Pallas kernels, put(): pl.pallas_call(put_body, out_shape=(jax.ShapeDtypeStruct(mixed.shape, mix...  3.38 us

profile of v4, /device:TPU:0, one launch (start us, length us, event | category | flops | bytes accessed | tf_op | source)
XLA Modules:
  0.0 62.0 jit_solution(2793976692815358841)
XLA Ops:
  0.6 58.0 %step.1 = (bf16[32,256]{1,0:T(8,128)(2,1)S(1)}, f32[2,32,4,64,64]{4,3,2,1,0:T(8,128)S(1)}) custom-call(bf16[32,256]{1,0:T(8,128)(2,1)} %tok.1, s32[1,32]{1,0:T(1,128)} %bitcast.15, f32[2,4096]{1,0:T(2,128)} %gain_hbm.1, f32[2,256]{1,0:T(2,128)} %base_hbm.1, f32[2,256]{1,0:T(2,128)} %rate_hbm.1, f32[2,256]{1,0:T(2,128)} %ggain_hbm.1, ...), custom_call_target="tpu_custom_call" | custom-call | tf_op jit(solution)/shard_map/step/pallas_call | solution.py:429
  58.6 3.4 %put.1 = (bf16[32,256]{1,0:T(8,128)(2,1)}, f32[2,32,4,64,64]{4,3,2,1,0:T(8,128)}) custom-call(bf16[32,256]{1,0:T(8,128)(2,1)S(1)} %get-tuple-element.4.mixed_ref, f32[2,32,4,64,64]{4,3,2,1,0:T(8,128)S(1)} %get-tuple-element.5.state_ref), custom_call_target="tpu_custom_call" | custom-call | tf_op jit(solution)/shard_map/put/pallas_call | solution.py:493

commit v5 on v4

--- a/solution.py
+++ b/solution.py
@@ -68,6 +68,9 @@
     def arrived(ref, sem):
         remote(ref, ref, ag_send.at[0], sem, t, sibling).wait_recv()
 
+    def fetched(ref, sem):
+        pltpu.make_async_copy(ref, ref, sem).wait()
+
     peers = [plane(o) for o in offs[1:]]
     far = peers[::-1]
     ks = [1, nx - 1] + list(range(2, nx - 1))
@@ -85,8 +88,11 @@
     def worow(dd, start=0, count=None):
         return pl.ds(pl.multiple_of(dd * slim + start, slim // 2), slim if count is None else count)
 
-    mine = pl.ds(pl.multiple_of(x * rows, rows), rows)
-    own_tok = fetch(tok, xg.at[0, t, mine], small_sem.at[5])
+    def slot(tt, xx, h, count=half):
+        start = tt * (nx * rows) + xx * rows + h * half
+        return pl.ds(pl.multiple_of(start, half), count)
+
+    own_tok = fetch(tok, xg.at[0, slot(t, x, 0, rows)], small_sem.at[5])
     barrier = pltpu.get_barrier_semaphore()
     everyone = [(p, d) for p in far] + [(t, 2 * o + core) for o in xs] + [(t, sibling)]
     for p in everyone:
@@ -98,8 +104,10 @@
         )
     ]
     own_s = [fetch(state.at[0], st.at[0], st_sem.at[0])]
-    own_w = [[fetch(weights[q].at[l], wcat.at[l, wrow(q)], own_sem.at[l, q]) for q in range(6)] for l in range(2)]
-    own_o = [fetch(wo.at[l], wot.at[l, worow(d)], own_sem.at[l, 6]) for l in range(2)]
+    for l in range(2):
+        for q in range(6):
+            fetch(weights[q].at[l], wcat.at[l, wrow(q)], own_sem.at[l])
+    own_o = [fetch(wo.at[l], wot.at[l, worow(d)], own_sem.at[2 + l]) for l in range(2)]
     own_s.append(fetch(state.at[1], st.at[1], st_sem.at[1]))
 
 
@@ -122,50 +130,45 @@
             copy.wait()
         own_tok.wait()
 
-    def own_rows(h, xx):
-        return pl.ds(pl.multiple_of(xx * rows + h * half, half), half)
-
-    def gather_start(l, source):
-        sent = []
-
-        def send(src, dst, rsem, tt, dd):
-            copy = remote(src, dst, ag_send.at[len(sent)], rsem, tt, dd)
-            copy.start()
-            sent.append(copy)
-
-        a_dst, b_dst = xg.at[l, t, own_rows(0, x)], xg.at[l, t, own_rows(1, x)]
+    def gather_start(l):
+        def send(block, rsem, tt, dd):
+            remote(block, block, ag_send.at[0], rsem, tt, dd).start()
+
+        first, second = xg.at[l, slot(t, x, 0)], xg.at[l, slot(t, x, 1)]
         for o in xs:
-            send(source(0), a_dst, a1_recv.at[l, x], t, 2 * o + core)
+            send(first, a1_recv.at[x], t, 2 * o + core)
         for p in far:
-            send(source(1), b_dst, b1_recv.at[l, t], p, d)
+            send(second, b1_recv.at[t], p, d)
         for p in far:
-            send(source(0), a_dst, fin_recv.at[l, t], p, d)
+            send(first, fin_recv.at[t], p, d)
         for o in xs:
-            send(source(1), b_dst, fin_recv.at[l, t], t, 2 * o + core)
-        return sent, send
+            send(second, fin_recv.at[t], t, 2 * o + core)
+        return send
 
     def gather_relay(l, send):
-        steps = [("a", o) for o in xs[:2]] + [("b", p) for p in peers[:4]]
-        steps += [("a", o) for o in xs[2:]] + [("b", p) for p in peers[4:]]
+        steps = [("b", peers[0]), ("a", xs[0])]
+        steps += [("b", peers[1]), ("a", xs[1])]
+        steps += [("b", p) for p in peers[2:4]] + [("a", o) for o in xs[2:]]
+        steps += [("b", p) for p in peers[4:]]
         for i, (kind, o) in enumerate(steps):
             with scope(f"{kind}{l}_{i}"):
                 if kind == "a":
-                    block = xg.at[l, t, own_rows(0, o)]
-                    arrived(block, a1_recv.at[l, o])
+                    block = xg.at[l, slot(t, o, 0)]
+                    arrived(block, a1_recv.at[o])
                     for p in far:
-                        send(block, block, fin_recv.at[l, t], p, d)
+                        send(block, fin_recv.at[t], p, d)
                 else:
-                    block = xg.at[l, o, own_rows(1, x)]
-                    arrived(block, b1_recv.at[l, o])
+                    block = xg.at[l, slot(o, x, 1)]
+                    arrived(block, b1_recv.at[o])
                     for p in xs:
-                        send(block, block, fin_recv.at[l, o], t, 2 * p + core)
+                        send(block, fin_recv.at[o], t, 2 * p + core)
+
+    def sent_all(ref, sem):
+        remote(ref, ref, sem, ex_recv.at[0], t, sibling).wait_send()
 
     def prepare(l):
-        for q in range(6):
-            own_w[l][q].wait()
-        for q in range(6):
-            other = pl.ds(pl.multiple_of(q * 2 * slim + (1 - core) * slim, slim), slim)
-            arrived(wcat.at[l, other], wc_recv.at[l, q])
+        fetched(wcat.at[l, pl.ds(0, 6 * slim)], own_sem.at[l])
+        arrived(wcat.at[l, pl.ds(0, 6 * slim)], wc_recv.at[l])
         line = gain[l : l + 1, :]
 
         def one(i, carry):
@@ -175,15 +178,17 @@
 
         lax.fori_loop(0, 12 * slim // 16, one, 0)
 
-    def project(l):
+    def project(l, after):
         acc[...] = jnp.zeros_like(acc)
         square[...] = jnp.zeros_like(square)
-        for o in offs:
+        for i, o in enumerate(offs):
             tt = plane(o)
             count = (nx - 1) * half if o == (0, 0) else (2 * nx - 1) * half
             with scope(f"x{l}_{o[0]}_{o[1]}"):
-                arrived(xg.at[l, tt, pl.ds(0, count)], fin_recv.at[l, tt])
-            block = xg[l, tt]
+                arrived(xg.at[l, pl.ds(0, count)], fin_recv.at[tt])
+            if i == 3:
+                after()
+            block = xg[l, slot(tt, 0, 0, nx * rows), :]
             cols = pl.ds(pl.multiple_of(tt * width, width), width)
             acc[...] += dot_t(block, wcat[l, :, cols])
             values = block.astype(jnp.float32)
@@ -196,13 +201,9 @@
         done = (acc[...] * factor).astype(jnp.bfloat16)
         for j in range(nx):
             pieces[l, j] = done[j * rows : (j + 1) * rows]
-        sent = []
-        for i, o in enumerate(xs):
-            copy = remote(pieces.at[l, o], vg.at[l, x], ex_send.at[l, i], ex_recv.at[l, x], t, 2 * o + core)
-            copy.start()
-            sent.append(copy)
+        for o in xs:
+            remote(pieces.at[l, o], vg.at[l, x], ex_send.at[0], ex_recv.at[x], t, 2 * o + core).start()
         vg[l, x] = pieces[l, x]
-        return sent
 
     part = slim // 2
     up, down, across = xpeer(1), xpeer(-1), xpeer(2)
@@ -211,49 +212,44 @@
         start, count = (0, slim) if piece is None else (piece * part, part)
         return wot.at[l, worow(2 * xx + cc, start, count)]
 
-    def out_send(l, sent, n, xx, piece, to_x, to_core):
+    def out_send(l, n, xx, piece, to_x, to_core):
         block = out_piece(l, xx, core, piece)
-        copy = remote(block, block, wo_send.at[l, n], wo_recv.at[l, n], t, 2 * to_x + to_core)
-        copy.start()
-        sent.append(copy)
-
-    def out_arrived(l, n, xx, piece, cc=None):
-        arrived(out_piece(l, xx, core if cc is None else cc, piece), wo_recv.at[l, n])
+        remote(block, block, wo_send.at[l], wo_recv.at[l, n], t, 2 * to_x + to_core).start()
+
+    def out_arrived(l, n, xx, piece):
+        arrived(out_piece(l, xx, core, piece), wo_recv.at[l, n])
 
     def out_first(l):
         own_o[l].wait()
-        sent = []
-        out_send(l, sent, 0, x, 0, up, core)
-        out_send(l, sent, 1, x, 1, down, core)
-        out_send(l, sent, 6, x, None, x, 1 - core)
-        return sent
-
-    def out_second(l, sent):
+        out_send(l, 0, x, 0, up, core)
+        out_send(l, 1, x, 1, down, core)
+        out_send(l, 6, x, None, x, 1 - core)
+
+    def out_second(l):
         out_arrived(l, 0, down, 0)
-        out_send(l, sent, 4, down, 0, up, core)
-        out_send(l, sent, 7, down, 0, x, 1 - core)
+        out_send(l, 4, down, 0, up, core)
+        out_send(l, 6, down, 0, x, 1 - core)
         out_arrived(l, 1, up, 1)
-        out_send(l, sent, 5, up, 1, down, core)
-        out_send(l, sent, 8, up, 1, x, 1 - core)
-
-    def out_third(l, sent):
-        out_send(l, sent, 2, x, 1, up, core)
-        out_send(l, sent, 3, x, 0, down, core)
-
-    def out_fourth(l, sent):
+        out_send(l, 5, up, 1, down, core)
+        out_send(l, 6, up, 1, x, 1 - core)
+
+    def out_third(l):
+        out_send(l, 2, x, 1, up, core)
+        out_send(l, 3, x, 0, down, core)
+
+    def out_fourth(l):
         out_arrived(l, 2, down, 1)
-        out_send(l, sent, 9, down, 1, x, 1 - core)
+        out_send(l, 6, down, 1, x, 1 - core)
         out_arrived(l, 3, up, 0)
-        out_send(l, sent, 10, up, 0, x, 1 - core)
-
-    def out_fifth(l, sent):
+        out_send(l, 6, up, 0, x, 1 - core)
+
+    def out_fifth(l):
         out_arrived(l, 4, across, 0)
         out_arrived(l, 5, across, 1)
-        out_send(l, sent, 11, across, None, x, 1 - core)
+        out_send(l, 6, across, None, x, 1 - core)
 
     def out_finish(l):
-        for n, xx, piece in ((6, x, None), (7, down, 0), (8, up, 1), (9, down, 1), (10, up, 0), (11, across, None)):
-            out_arrived(l, n, xx, piece, 1 - core)
+        arrived(wot.at[l, pl.ds(0, nx * slim)], wo_recv.at[l, 6])
 
     size = 2 * slim
     sub = lax.broadcasted_iota(jnp.int32, (rows, rows), 0)
@@ -282,7 +278,7 @@
                 update(0)
         with scope(f"exchange{l}"):
             for o in xs:
-                arrived(vg.at[l, o], ex_recv.at[l, o])
+                arrived(vg.at[l, o], ex_recv.at[o])
         looks, extras, gates = [], [], []
         for h in range(nx):
             part = slice(h * size, (h + 1) * size)
@@ -304,7 +300,6 @@
             gates.append(jax.nn.sigmoid(gate_pre) * ggain[l : l + 1, part])
         gates = [paired(gates, p) for p in range(nx // 2)]
         extras = [paired(extras, p) for p in range(nx // 2)]
-        sent = []
         for g in range(2):
             reads = [[] for p in range(nx // 2)]
             for k in range(half // 8):
@@ -327,14 +322,11 @@
                 apart = read - by_head(read)
                 normal = apart * lax.rsqrt(by_head(apart * apart) + GROUP_EPS) * gates[p][span]
                 outs.append(jnp.where(live[span], normal, 0.0).astype(jnp.bfloat16))
-            span = pl.ds(g * half, half)
-            mg[l, t, span, :] = jnp.concatenate(outs, axis=1)
-            block = mg.at[l, t, span]
-            for i, p in enumerate(far):
-                copy = remote(block, block, mg_send.at[l, g * (tp - 1) + i], mg_recv.at[l, t], p, d)
-                copy.start()
-                sent.append(copy)
-        return sent
+            span = pl.ds(pl.multiple_of(t * rows + g * half, half), half)
+            mg[l, span, :] = jnp.concatenate(outs, axis=1)
+            block = mg.at[l, span]
+            for p in far:
+                remote(block, block, mg_send.at[0], mg_recv.at[t], p, d).start()
 
     eye = lax.broadcasted_iota(jnp.int32, (size, size), 0) == lax.broadcasted_iota(jnp.int32, (size, size), 1)
 
@@ -355,32 +347,28 @@
         total = jnp.zeros((rows, width), jnp.float32)
         for o in offs:
             tt = plane(o)
+            span = pl.ds(pl.multiple_of(tt * rows, rows), rows)
             if o != (0, 0):
                 with scope(f"m{l}_{o[0]}_{o[1]}"):
-                    arrived(mg.at[l, tt], mg_recv.at[l, tt])
+                    arrived(mg.at[l, span], mg_recv.at[tt])
             cols = pl.ds(pl.multiple_of(tt * width, width), width)
-            total += dot_t(mg[l, tt], wot[l, :, cols])
+            total += dot_t(mg[l, span, :], wot[l, :, cols])
         return total.astype(jnp.bfloat16)
 
     for l in range(2):
         with scope(f"start{l}"):
             if l == 1:
-                xg[1, t, mine, :] = current
-            sent, send = gather_start(l, lambda h: xg.at[l, t, own_rows(h, x)])
+                xg[1, slot(t, x, 0, rows), :] = current
+            send = gather_start(l)
             if l == 0:
-                shared = []
                 for ll in range(2):
                     for q in range(6):
-                        copy = remote(
-                            weights[q].at[ll], wcat.at[ll, wrow(q)],
-                            wc_send.at[ll, q], wc_recv.at[ll, q], t, sibling,
-                        )
-                        copy.start()
-                        shared.append(copy)
-            if l == 0:
-                folded = [out_first(0)]
+                        remote(
+                            weights[q].at[ll], wcat.at[ll, wrow(q)], wc_send.at[0], wc_recv.at[ll], t, sibling
+                        ).start()
+                out_first(0)
             else:
-                out_second(1, folded[1])
+                out_second(1)
         if l == 0:
             with scope("turn0"):
                 turn(0)
@@ -389,20 +377,16 @@
             with scope("prepare0"):
                 prepare(0)
         with scope(f"project{l}"):
-            traded = project(l)
-            out_third(l, folded[l])
+            project(l, lambda: out_second(0) if l == 0 else None)
+            out_third(l)
+            sent_all(xg.at[l, pl.ds(0, ((nx - 1) * (tp + 1) + (tp - 1) * (nx + 1)) * half)], ag_send.at[0])
+        with scope(f"recur{l}"):
+            recur(l)
+        with scope(f"outfourth{l}"):
+            out_fourth(l)
             if l == 0:
-                out_second(0, folded[0])
-            for copy in sent:
-                copy.wait_send()
-        with scope(f"recur{l}"):
-            mixed = recur(l)
-        with scope(f"outfourth{l}"):
-            out_fourth(l, folded[l])
-            if l == 0:
-                folded.append(out_first(1))
-        with scope(f"outfifth{l}"):
-            out_fifth(l, folded[l])
+                out_first(1)
+            out_fifth(l)
         if l == 1:
             with scope("update1"):
                 update(1)
@@ -410,11 +394,11 @@
             out_finish(l)
         with scope(f"fold{l}"):
             current = fold(l)
-        for copy in traded + folded[l] + mixed:
-            copy.wait_send()
+        sent_all(pieces.at[l, pl.ds(0, nx - 1)], ex_send.at[0])
+        sent_all(mg.at[l, pl.ds(0, (tp - 1) * rows)], mg_send.at[0])
+        sent_all(wot.at[l, pl.ds(0, 7 * slim)], wo_send.at[l])
     mixed_ref[...] = current
-    for copy in shared:
-        copy.wait_send()
+    sent_all(wcat.at[0], wc_send.at[0])
 
 
 def step(tok, lens, gain, base, rate, ggain, weights, wo, state, tp, dp):
@@ -435,11 +419,11 @@
         in_specs=[hbm] * 14,
         out_specs=(vmem, vmem),
         scratch_shapes=[
-            pltpu.VMEM((2, tp, nx * rows, width), bf),
+            pltpu.VMEM((2, tp * nx * rows, width), bf),
             pltpu.VMEM((2, 12 * slim, feat), bf),
             pltpu.VMEM((2, width, feat), bf),
             pltpu.VMEM((2, nx, rows, 12 * slim), bf),
-            pltpu.VMEM((2, tp, rows, width), bf),
+            pltpu.VMEM((2, tp * rows, width), bf),
             pltpu.VMEM((2, nx, rows, 12 * slim), bf),
             pltpu.VMEM((2, rows, 2 * slim, nx * 2 * slim), bf),
             pltpu.VMEM((2, 4, nx, rows, 2 * slim), jnp.float32),
@@ -450,19 +434,19 @@
             pltpu.VMEM(base.shape, base.dtype),
             pltpu.VMEM(rate.shape, rate.dtype),
             pltpu.VMEM(ggain.shape, ggain.dtype),
-            dma(((nx - 1) * (tp + 1) + (tp - 1) * (nx + 1),)),
-            dma((2, nx)),
-            dma((2, tp)),
-            dma((2, tp)),
-            dma((2, nx)),
-            dma((2, nx)),
-            dma((2, 2 * tp)),
-            dma((2, tp)),
-            dma((2, 12)),
-            dma((2, 12)),
-            dma((2, 6)),
-            dma((2, 6)),
+            dma((1,)),
+            dma((nx,)),
+            dma((tp,)),
+            dma((tp,)),
+            dma((1,)),
+            dma((nx,)),
+            dma((1,)),
+            dma((tp,)),
+            dma((2,)),
             dma((2, 7)),
+            dma((1,)),
+            dma((2,)),
+            dma((4,)),
             dma((2,)),
             dma((6,)),
         ],

time: 62.1 us -> 58 us (0.934)
  Pallas kernels: 61.4 us -> 57.3 us
    pallas_call x1, Pallas kernels: 58 us -> 53.9 us  [step(): pl.pallas_call(functools.partial(step_body, tp=tp, dp=dp), out_shape=(plt...]
where the time goes in v5:
time: 58 us; the launch traced here: 57.9 us
  Pallas kernels  57.3 us (99%)
  between operations  0.64 us (1%)
    pallas_call x1, Pallas kernels, step(): pl.pallas_call(functools.partial(step_body, tp=tp, dp=dp), out_shape=(plt...  53.9 us
    pallas_call x1, Pallas kernels, put(): pl.pallas_call(put_body, out_shape=(jax.ShapeDtypeStruct(mixed.shape, mix...  3.38 us

profile of v5, /device:TPU:0, one launch (start us, length us, event | category | flops | bytes accessed | tf_op | source)
XLA Modules:
  0.0 57.9 jit_solution(273578708184094420)
XLA Ops:
  0.6 53.9 %step.1 = (bf16[32,256]{1,0:T(8,128)(2,1)S(1)}, f32[2,32,4,64,64]{4,3,2,1,0:T(8,128)S(1)}) custom-call(bf16[32,256]{1,0:T(8,128)(2,1)} %tok.1, s32[1,32]{1,0:T(1,128)} %bitcast.15, f32[2,4096]{1,0:T(2,128)} %gain_hbm.1, f32[2,256]{1,0:T(2,128)} %base_hbm.1, f32[2,256]{1,0:T(2,128)} %rate_hbm.1, f32[2,256]{1,0:T(2,128)} %ggain_hbm.1, ...), custom_call_target="tpu_custom_call" | custom-call | tf_op jit(solution)/shard_map/step/pallas_call | solution.py:413
  54.6 3.4 %put.1 = (bf16[32,256]{1,0:T(8,128)(2,1)}, f32[2,32,4,64,64]{4,3,2,1,0:T(8,128)}) custom-call(bf16[32,256]{1,0:T(8,128)(2,1)S(1)} %get-tuple-element.4.mixed_ref, f32[2,32,4,64,64]{4,3,2,1,0:T(8,128)S(1)} %get-tuple-element.5.state_ref), custom_call_target="tpu_custom_call" | custom-call | tf_op jit(solution)/shard_map/put/pallas_call | solution.py:477

commit v6 on v5

--- a/solution.py
+++ b/solution.py
@@ -85,9 +85,6 @@
     def wrow(q):
         return pl.ds(pl.multiple_of(q * 2 * slim + core * slim, slim), slim)
 
-    def worow(dd, start=0, count=None):
-        return pl.ds(pl.multiple_of(dd * slim + start, slim // 2), slim if count is None else count)
-
     def slot(tt, xx, h, count=half):
         start = tt * (nx * rows) + xx * rows + h * half
         return pl.ds(pl.multiple_of(start, half), count)
@@ -97,6 +94,7 @@
     everyone = [(p, d) for p in far] + [(t, 2 * o + core) for o in xs] + [(t, sibling)]
     for p in everyone:
         pl.semaphore_signal(barrier, inc=1, device_id=p, device_id_type=MESH)
+    own_tok.wait()
     small = [
         fetch(src, dst, small_sem.at[i])
         for i, (src, dst) in enumerate(
@@ -107,7 +105,10 @@
     for l in range(2):
         for q in range(6):
             fetch(weights[q].at[l], wcat.at[l, wrow(q)], own_sem.at[l])
-    own_o = [fetch(wo.at[l], wot.at[l, worow(d)], own_sem.at[2 + l]) for l in range(2)]
+    own_o = [
+        fetch(wo.at[l], wot.at[pl.ds(pl.multiple_of(l * width + d * slim, slim), slim)], own_sem.at[2 + l])
+        for l in range(2)
+    ]
     own_s.append(fetch(state.at[1], st.at[1], st_sem.at[1]))
 
 
@@ -125,10 +126,6 @@
 
     with scope("barrier"):
         pl.semaphore_wait(barrier, len(everyone))
-    with scope("small"):
-        for copy in small:
-            copy.wait()
-        own_tok.wait()
 
     def gather_start(l):
         def send(block, rsem, tt, dd):
@@ -146,11 +143,11 @@
         return send
 
     def gather_relay(l, send):
-        steps = [("b", peers[0]), ("a", xs[0])]
-        steps += [("b", peers[1]), ("a", xs[1])]
-        steps += [("b", p) for p in peers[2:4]] + [("a", o) for o in xs[2:]]
-        steps += [("b", p) for p in peers[4:]]
+        steps = [("a", o) for o in xs[:2]] + [("b", p) for p in peers[:4]]
+        steps += [("a", o) for o in xs[2:]] + [("b", p) for p in peers[4:]]
         for i, (kind, o) in enumerate(steps):
+            if l == 0 and i == 4:
+                out_first(0)
             with scope(f"{kind}{l}_{i}"):
                 if kind == "a":
                     block = xg.at[l, slot(t, o, 0)]
@@ -181,7 +178,7 @@
     def project(l, after):
         acc[...] = jnp.zeros_like(acc)
         square[...] = jnp.zeros_like(square)
-        for i, o in enumerate(offs):
+        for i, o in enumerate(offs[:1] + offs[:0:-1]):
             tt = plane(o)
             count = (nx - 1) * half if o == (0, 0) else (2 * nx - 1) * half
             with scope(f"x{l}_{o[0]}_{o[1]}"):
@@ -205,57 +202,73 @@
             remote(pieces.at[l, o], vg.at[l, x], ex_send.at[0], ex_recv.at[x], t, 2 * o + core).start()
         vg[l, x] = pieces[l, x]
 
-    part = slim // 2
     up, down, across = xpeer(1), xpeer(-1), xpeer(2)
 
-    def out_piece(l, xx, cc, piece):
-        start, count = (0, slim) if piece is None else (piece * part, part)
-        return wot.at[l, worow(2 * xx + cc, start, count)]
-
-    def out_send(l, n, xx, piece, to_x, to_core):
-        block = out_piece(l, xx, core, piece)
+    def block_of(l, xx, cc):
+        return wot.at[pl.ds(pl.multiple_of(l * width + (2 * xx + cc) * slim, slim), slim)]
+
+    def out_send(l, n, xx, cc, to_x, to_core):
+        block = block_of(l, xx, cc)
         remote(block, block, wo_send.at[l], wo_recv.at[l, n], t, 2 * to_x + to_core).start()
 
-    def out_arrived(l, n, xx, piece):
-        arrived(out_piece(l, xx, core, piece), wo_recv.at[l, n])
+    def out_arrived(l, n, count=1):
+        arrived(wot.at[pl.ds(0, count * slim)], wo_recv.at[l, n])
+
+    def ring(body):
+        pl.when(core == 1)(body)
 
     def out_first(l):
         own_o[l].wait()
-        out_send(l, 0, x, 0, up, core)
-        out_send(l, 1, x, 1, down, core)
-        out_send(l, 6, x, None, x, 1 - core)
+
+        @ring
+        def _():
+            out_arrived(l, 6)
+            out_send(l, 0, x, 0, up, 1)
+            out_send(l, 1, x, 1, down, 1)
 
     def out_second(l):
-        out_arrived(l, 0, down, 0)
-        out_send(l, 4, down, 0, up, core)
-        out_send(l, 6, down, 0, x, 1 - core)
-        out_arrived(l, 1, up, 1)
-        out_send(l, 5, up, 1, down, core)
-        out_send(l, 6, up, 1, x, 1 - core)
+        @ring
+        def _():
+            out_arrived(l, 0)
+            out_send(l, 4, down, 0, up, 1)
+            out_send(l, 6, down, 0, x, 0)
+            out_arrived(l, 1)
+            out_send(l, 5, up, 1, down, 1)
+            out_send(l, 6, up, 1, x, 0)
 
     def out_third(l):
-        out_send(l, 2, x, 1, up, core)
-        out_send(l, 3, x, 0, down, core)
+        @ring
+        def _():
+            out_send(l, 2, x, 1, up, 1)
+            out_send(l, 3, x, 0, down, 1)
 
     def out_fourth(l):
-        out_arrived(l, 2, down, 1)
-        out_send(l, 6, down, 1, x, 1 - core)
-        out_arrived(l, 3, up, 0)
-        out_send(l, 6, up, 0, x, 1 - core)
-
-    def out_fifth(l):
-        out_arrived(l, 4, across, 0)
-        out_arrived(l, 5, across, 1)
-        out_send(l, 6, across, None, x, 1 - core)
+        @ring
+        def _():
+            out_arrived(l, 4)
+            out_send(l, 6, across, 0, x, 0)
+            out_arrived(l, 5)
+            out_send(l, 6, across, 1, x, 0)
+            out_arrived(l, 2)
+            out_send(l, 6, down, 1, x, 0)
+            out_arrived(l, 3)
+            out_send(l, 6, up, 0, x, 0)
 
     def out_finish(l):
-        arrived(wot.at[l, pl.ds(0, nx * slim)], wo_recv.at[l, 6])
+        @pl.when(core == 0)
+        def _():
+            out_arrived(l, 6, 2 * nx - 1)
+
+    def out_done(l):
+        @ring
+        def _():
+            sent_all(wot.at[pl.ds(0, 13 * slim)], wo_send.at[l])
+
+        @pl.when(core == 0)
+        def _():
+            sent_all(wot.at[pl.ds(0, slim)], wo_send.at[l])
 
     size = 2 * slim
-    sub = lax.broadcasted_iota(jnp.int32, (rows, rows), 0)
-    lane = lax.broadcasted_iota(jnp.int32, (rows, rows), 1)
-    spread = jnp.where(sub == lane, lens[...].astype(jnp.float32), 0.0)
-    live = jnp.sum(spread, axis=1, keepdims=True) > STEP
     eight = lax.broadcasted_iota(jnp.int32, (8, 2 * size), 0)
     left = lax.broadcasted_iota(jnp.int32, (8, 2 * size), 1) < size
     left_half = lax.broadcasted_iota(jnp.int32, (half, 2 * size), 1) < size
@@ -279,6 +292,10 @@
         with scope(f"exchange{l}"):
             for o in xs:
                 arrived(vg.at[l, o], ex_recv.at[o])
+        sub = lax.broadcasted_iota(jnp.int32, (rows, rows), 0)
+        lane = lax.broadcasted_iota(jnp.int32, (rows, rows), 1)
+        spread = jnp.where(sub == lane, lens[...].astype(jnp.float32), 0.0)
+        live = jnp.sum(spread, axis=1, keepdims=True) > STEP
         looks, extras, gates = [], [], []
         for h in range(nx):
             part = slice(h * size, (h + 1) * size)
@@ -345,14 +362,14 @@
 
     def fold(l):
         total = jnp.zeros((rows, width), jnp.float32)
-        for o in offs:
+        for o in offs[:1] + offs[:0:-1]:
             tt = plane(o)
             span = pl.ds(pl.multiple_of(tt * rows, rows), rows)
             if o != (0, 0):
                 with scope(f"m{l}_{o[0]}_{o[1]}"):
                     arrived(mg.at[l, span], mg_recv.at[tt])
             cols = pl.ds(pl.multiple_of(tt * width, width), width)
-            total += dot_t(mg[l, span, :], wot[l, :, cols])
+            total += dot_t(mg[l, span, :], wot[pl.ds(l * width, width), cols])
         return total.astype(jnp.bfloat16)
 
     for l in range(2):
@@ -362,11 +379,15 @@
             send = gather_start(l)
             if l == 0:
                 for ll in range(2):
+                    remote(
+                        wo.at[ll],
+                        wot.at[pl.ds(pl.multiple_of(ll * width + d * slim, slim), slim)],
+                        wo_send.at[ll], wo_recv.at[ll, 6], t, sibling,
+                    ).start()
                     for q in range(6):
                         remote(
                             weights[q].at[ll], wcat.at[ll, wrow(q)], wc_send.at[0], wc_recv.at[ll], t, sibling
                         ).start()
-                out_first(0)
             else:
                 out_second(1)
         if l == 0:
@@ -375,6 +396,8 @@
         gather_relay(l, send)
         if l == 0:
             with scope("prepare0"):
+                for copy in small:
+                    copy.wait()
                 prepare(0)
         with scope(f"project{l}"):
             project(l, lambda: out_second(0) if l == 0 else None)
@@ -386,7 +409,6 @@
             out_fourth(l)
             if l == 0:
                 out_first(1)
-            out_fifth(l)
         if l == 1:
             with scope("update1"):
                 update(1)
@@ -396,7 +418,7 @@
             current = fold(l)
         sent_all(pieces.at[l, pl.ds(0, nx - 1)], ex_send.at[0])
         sent_all(mg.at[l, pl.ds(0, (tp - 1) * rows)], mg_send.at[0])
-        sent_all(wot.at[l, pl.ds(0, 7 * slim)], wo_send.at[l])
+        out_done(l)
     mixed_ref[...] = current
     sent_all(wcat.at[0], wc_send.at[0])
 
@@ -421,7 +443,7 @@
         scratch_shapes=[
             pltpu.VMEM((2, tp * nx * rows, width), bf),
             pltpu.VMEM((2, 12 * slim, feat), bf),
-            pltpu.VMEM((2, width, feat), bf),
+            pltpu.VMEM((2 * width, feat), bf),
             pltpu.VMEM((2, nx, rows, 12 * slim), bf),
             pltpu.VMEM((2, tp * rows, width), bf),
             pltpu.VMEM((2, nx, rows, 12 * slim), bf),

time: 58 us -> 65.5 us (1.13)
  Pallas kernels: 57.3 us -> 64.7 us
    pallas_call x1, Pallas kernels: 53.9 us -> 61.3 us  [step(): pl.pallas_call(functools.partial(step_body, tp=tp, dp=dp), out_shape=(plt...]
where the time goes in v6:
time: 65.5 us; the launch traced here: 65.3 us
  Pallas kernels  64.7 us (99%)
    pallas_call x1, Pallas kernels, step(): pl.pallas_call(functools.partial(step_body, tp=tp, dp=dp), out_shape=(plt...  61.3 us
    pallas_call x1, Pallas kernels, put(): pl.pallas_call(put_body, out_shape=(jax.ShapeDtypeStruct(mixed.shape, mix...  3.38 us

profile of v6, /device:TPU:0, one launch (start us, length us, event | category | flops | bytes accessed | tf_op | source)
XLA Modules:
  0.0 65.3 jit_solution(3587392343339435472)
XLA Ops:
  0.6 61.3 %step.1 = (bf16[32,256]{1,0:T(8,128)(2,1)S(1)}, f32[2,32,4,64,64]{4,3,2,1,0:T(8,128)S(1)}) custom-call(bf16[32,256]{1,0:T(8,128)(2,1)} %tok.1, s32[1,32]{1,0:T(1,128)} %bitcast.15, f32[2,4096]{1,0:T(2,128)} %gain_hbm.1, f32[2,256]{1,0:T(2,128)} %base_hbm.1, f32[2,256]{1,0:T(2,128)} %rate_hbm.1, f32[2,256]{1,0:T(2,128)} %ggain_hbm.1, ...), custom_call_target="tpu_custom_call" | custom-call | tf_op jit(solution)/shard_map/step/pallas_call | solution.py:435
  61.9 3.4 %put.1 = (bf16[32,256]{1,0:T(8,128)(2,1)}, f32[2,32,4,64,64]{4,3,2,1,0:T(8,128)}) custom-call(bf16[32,256]{1,0:T(8,128)(2,1)S(1)} %get-tuple-element.4.mixed_ref, f32[2,32,4,64,64]{4,3,2,1,0:T(8,128)S(1)} %get-tuple-element.5.state_ref), custom_call_target="tpu_custom_call" | custom-call | tf_op jit(solution)/shard_map/put/pallas_call | solution.py:499

commit v7 on v5

--- a/solution.py
+++ b/solution.py
@@ -126,8 +126,6 @@
     with scope("barrier"):
         pl.semaphore_wait(barrier, len(everyone))
     with scope("small"):
-        for copy in small:
-            copy.wait()
         own_tok.wait()
 
     def gather_start(l):
@@ -252,10 +250,6 @@
         arrived(wot.at[l, pl.ds(0, nx * slim)], wo_recv.at[l, 6])
 
     size = 2 * slim
-    sub = lax.broadcasted_iota(jnp.int32, (rows, rows), 0)
-    lane = lax.broadcasted_iota(jnp.int32, (rows, rows), 1)
-    spread = jnp.where(sub == lane, lens[...].astype(jnp.float32), 0.0)
-    live = jnp.sum(spread, axis=1, keepdims=True) > STEP
     eight = lax.broadcasted_iota(jnp.int32, (8, 2 * size), 0)
     left = lax.broadcasted_iota(jnp.int32, (8, 2 * size), 1) < size
     left_half = lax.broadcasted_iota(jnp.int32, (half, 2 * size), 1) < size
@@ -279,6 +273,10 @@
         with scope(f"exchange{l}"):
             for o in xs:
                 arrived(vg.at[l, o], ex_recv.at[o])
+        sub = lax.broadcasted_iota(jnp.int32, (rows, rows), 0)
+        lane = lax.broadcasted_iota(jnp.int32, (rows, rows), 1)
+        spread = jnp.where(sub == lane, lens[...].astype(jnp.float32), 0.0)
+        live = jnp.sum(spread, axis=1, keepdims=True) > STEP
         looks, extras, gates = [], [], []
         for h in range(nx):
             part = slice(h * size, (h + 1) * size)
@@ -375,6 +373,8 @@
         gather_relay(l, send)
         if l == 0:
             with scope("prepare0"):
+                for copy in small:
+                    copy.wait()
                 prepare(0)
         with scope(f"project{l}"):
             project(l, lambda: out_second(0) if l == 0 else None)

time: 58 us -> 57.6 us (level)
  no operation moved by 1% of the time
where the time goes in v7:
time: 57.6 us; the launch traced here: 57.5 us
  Pallas kernels  56.9 us (99%)
  between operations  0.64 us (1%)
    pallas_call x1, Pallas kernels, step(): pl.pallas_call(functools.partial(step_body, tp=tp, dp=dp), out_shape=(plt...  53.5 us
    pallas_call x1, Pallas kernels, put(): pl.pallas_call(put_body, out_shape=(jax.ShapeDtypeStruct(mixed.shape, mix...  3.38 us

profile of v7, /device:TPU:0, one launch (start us, length us, event | category | flops | bytes accessed | tf_op | source)
XLA Modules:
  0.0 57.5 jit_solution(273239081789115266)
XLA Ops:
  0.6 53.5 %step.1 = (bf16[32,256]{1,0:T(8,128)(2,1)S(1)}, f32[2,32,4,64,64]{4,3,2,1,0:T(8,128)S(1)}) custom-call(bf16[32,256]{1,0:T(8,128)(2,1)} %tok.1, s32[1,32]{1,0:T(1,128)} %bitcast.15, f32[2,4096]{1,0:T(2,128)} %gain_hbm.1, f32[2,256]{1,0:T(2,128)} %base_hbm.1, f32[2,256]{1,0:T(2,128)} %rate_hbm.1, f32[2,256]{1,0:T(2,128)} %ggain_hbm.1, ...), custom_call_target="tpu_custom_call" | custom-call | tf_op jit(solution)/shard_map/step/pallas_call | solution.py:413
  54.1 3.4 %put.1 = (bf16[32,256]{1,0:T(8,128)(2,1)}, f32[2,32,4,64,64]{4,3,2,1,0:T(8,128)}) custom-call(bf16[32,256]{1,0:T(8,128)(2,1)S(1)} %get-tuple-element.4.mixed_ref, f32[2,32,4,64,64]{4,3,2,1,0:T(8,128)S(1)} %get-tuple-element.5.state_ref), custom_call_target="tpu_custom_call" | custom-call | tf_op jit(solution)/shard_map/put/pallas_call | solution.py:477

commit v8 on v7

--- a/solution.py
+++ b/solution.py
@@ -13,6 +13,7 @@
 GROUP_EPS = 0.00064
 VMEM_LIMIT = 55_000_000
 MESH = pl.DeviceIdType.MESH
+CUT = (16, 16)
 
 
 def scope(name):
@@ -72,9 +73,10 @@
         pltpu.make_async_copy(ref, ref, sem).wait()
 
     peers = [plane(o) for o in offs[1:]]
-    far = peers[::-1]
+    far = peers
     ks = [1, nx - 1] + list(range(2, nx - 1))
     xs = [xpeer(k) for k in ks]
+    outward = xs[::-1]
 
 
     def fetch(src, dst, sem):
@@ -88,11 +90,14 @@
     def worow(dd, start=0, count=None):
         return pl.ds(pl.multiple_of(dd * slim + start, slim // 2), slim if count is None else count)
 
-    def slot(tt, xx, h, count=half):
-        start = tt * (nx * rows) + xx * rows + h * half
-        return pl.ds(pl.multiple_of(start, half), count)
-
-    own_tok = fetch(tok, xg.at[0, slot(t, x, 0, rows)], small_sem.at[5])
+    def slot(tt, xx, count):
+        return pl.ds(pl.multiple_of(tt * (nx * rows) + xx * rows, rows), count)
+
+    def share(l, tt, xx, h):
+        start, count = (0, CUT[l]) if h == 0 else (CUT[l], rows - CUT[l])
+        return pl.ds(pl.multiple_of(tt * (nx * rows) + xx * rows + start, 8), count)
+
+    own_tok = fetch(tok, xg.at[0, slot(t, x, rows)], small_sem.at[5])
     barrier = pltpu.get_barrier_semaphore()
     everyone = [(p, d) for p in far] + [(t, 2 * o + core) for o in xs] + [(t, sibling)]
     for p in everyone:
@@ -132,15 +137,15 @@
         def send(block, rsem, tt, dd):
             remote(block, block, ag_send.at[0], rsem, tt, dd).start()
 
-        first, second = xg.at[l, slot(t, x, 0)], xg.at[l, slot(t, x, 1)]
-        for o in xs:
+        first, second = xg.at[l, share(l, t, x, 0)], xg.at[l, share(l, t, x, 1)]
+        for o in outward:
             send(first, a1_recv.at[x], t, 2 * o + core)
-        for p in far:
+        for p in peers:
             send(second, b1_recv.at[t], p, d)
+        for o in outward:
+            send(second, fin_recv.at[t], t, 2 * o + core)
         for p in far:
             send(first, fin_recv.at[t], p, d)
-        for o in xs:
-            send(second, fin_recv.at[t], t, 2 * o + core)
         return send
 
     def gather_relay(l, send):
@@ -151,14 +156,14 @@
         for i, (kind, o) in enumerate(steps):
             with scope(f"{kind}{l}_{i}"):
                 if kind == "a":
-                    block = xg.at[l, slot(t, o, 0)]
+                    block = xg.at[l, share(l, t, o, 0)]
                     arrived(block, a1_recv.at[o])
                     for p in far:
                         send(block, fin_recv.at[t], p, d)
                 else:
-                    block = xg.at[l, slot(o, x, 1)]
+                    block = xg.at[l, share(l, o, x, 1)]
                     arrived(block, b1_recv.at[o])
-                    for p in xs:
+                    for p in outward:
                         send(block, fin_recv.at[o], t, 2 * p + core)
 
     def sent_all(ref, sem):
@@ -181,12 +186,12 @@
         square[...] = jnp.zeros_like(square)
         for i, o in enumerate(offs):
             tt = plane(o)
-            count = (nx - 1) * half if o == (0, 0) else (2 * nx - 1) * half
+            count = (nx - 1) * (rows - CUT[l]) + (0 if o == (0, 0) else nx * CUT[l])
             with scope(f"x{l}_{o[0]}_{o[1]}"):
                 arrived(xg.at[l, pl.ds(0, count)], fin_recv.at[tt])
             if i == 3:
                 after()
-            block = xg[l, slot(tt, 0, 0, nx * rows), :]
+            block = xg[l, slot(tt, 0, nx * rows), :]
             cols = pl.ds(pl.multiple_of(tt * width, width), width)
             acc[...] += dot_t(block, wcat[l, :, cols])
             values = block.astype(jnp.float32)
@@ -199,7 +204,7 @@
         done = (acc[...] * factor).astype(jnp.bfloat16)
         for j in range(nx):
             pieces[l, j] = done[j * rows : (j + 1) * rows]
-        for o in xs:
+        for o in outward:
             remote(pieces.at[l, o], vg.at[l, x], ex_send.at[0], ex_recv.at[x], t, 2 * o + core).start()
         vg[l, x] = pieces[l, x]
 
@@ -356,7 +361,7 @@
     for l in range(2):
         with scope(f"start{l}"):
             if l == 1:
-                xg[1, slot(t, x, 0, rows), :] = current
+                xg[1, slot(t, x, rows), :] = current
             send = gather_start(l)
             if l == 0:
                 for ll in range(2):
@@ -379,7 +384,8 @@
         with scope(f"project{l}"):
             project(l, lambda: out_second(0) if l == 0 else None)
             out_third(l)
-            sent_all(xg.at[l, pl.ds(0, ((nx - 1) * (tp + 1) + (tp - 1) * (nx + 1)) * half)], ag_send.at[0])
+            count = ((nx - 1) + (tp - 1) * nx) * CUT[l] + ((tp - 1) + tp * (nx - 1)) * (rows - CUT[l])
+            sent_all(xg.at[l, pl.ds(0, count)], ag_send.at[0])
         with scope(f"recur{l}"):
             recur(l)
         with scope(f"outfourth{l}"):

time: 57.6 us -> 56.9 us (0.988)
  Pallas kernels: 56.9 us -> 56.1 us
    pallas_call x1, Pallas kernels: 53.5 us -> 52.7 us  [step(): pl.pallas_call(functools.partial(step_body, tp=tp, dp=dp), out_shape=(plt...]
where the time goes in v8:
time: 56.9 us; the launch traced here: 56.8 us
  Pallas kernels  56.1 us (99%)
  between operations  0.64 us (1%)
    pallas_call x1, Pallas kernels, step(): pl.pallas_call(functools.partial(step_body, tp=tp, dp=dp), out_shape=(plt...  52.7 us
    pallas_call x1, Pallas kernels, put(): pl.pallas_call(put_body, out_shape=(jax.ShapeDtypeStruct(mixed.shape, mix...  3.38 us

profile of v8, /device:TPU:0, one launch (start us, length us, event | category | flops | bytes accessed | tf_op | source)
XLA Modules:
  0.0 56.8 jit_solution(15467728066791618079)
XLA Ops:
  0.6 52.7 %step.1 = (bf16[32,256]{1,0:T(8,128)(2,1)S(1)}, f32[2,32,4,64,64]{4,3,2,1,0:T(8,128)S(1)}) custom-call(bf16[32,256]{1,0:T(8,128)(2,1)} %tok.1, s32[1,32]{1,0:T(1,128)} %bitcast.15, f32[2,4096]{1,0:T(2,128)} %gain_hbm.1, f32[2,256]{1,0:T(2,128)} %base_hbm.1, f32[2,256]{1,0:T(2,128)} %rate_hbm.1, f32[2,256]{1,0:T(2,128)} %ggain_hbm.1, ...), custom_call_target="tpu_custom_call" | custom-call | tf_op jit(solution)/shard_map/step/pallas_call | solution.py:419
  53.4 3.4 %put.1 = (bf16[32,256]{1,0:T(8,128)(2,1)}, f32[2,32,4,64,64]{4,3,2,1,0:T(8,128)}) custom-call(bf16[32,256]{1,0:T(8,128)(2,1)S(1)} %get-tuple-element.4.mixed_ref, f32[2,32,4,64,64]{4,3,2,1,0:T(8,128)S(1)} %get-tuple-element.5.state_ref), custom_call_target="tpu_custom_call" | custom-call | tf_op jit(solution)/shard_map/put/pallas_call | solution.py:483

commit v9 on v8

--- a/solution.py
+++ b/solution.py
@@ -99,20 +99,21 @@
 
     own_tok = fetch(tok, xg.at[0, slot(t, x, rows)], small_sem.at[5])
     barrier = pltpu.get_barrier_semaphore()
-    everyone = [(p, d) for p in far] + [(t, 2 * o + core) for o in xs] + [(t, sibling)]
+    everyone = [(p, d) for p in far[::-1]] + [(t, 2 * o + core) for o in xs] + [(t, sibling)]
     for p in everyone:
         pl.semaphore_signal(barrier, inc=1, device_id=p, device_id_type=MESH)
+    own_o = [fetch(wo.at[0], wot.at[0, worow(d)], own_sem.at[2])]
     small = [
         fetch(src, dst, small_sem.at[i])
         for i, (src, dst) in enumerate(
             [(lens_hbm, lens), (gain_hbm, gain), (base_hbm, base), (rate_hbm, rate), (ggain_hbm, ggain)]
         )
     ]
-    own_s = [fetch(state.at[0], st.at[0], st_sem.at[0])]
     for l in range(2):
         for q in range(6):
             fetch(weights[q].at[l], wcat.at[l, wrow(q)], own_sem.at[l])
-    own_o = [fetch(wo.at[l], wot.at[l, worow(d)], own_sem.at[2 + l]) for l in range(2)]
+    own_s = [fetch(state.at[0], st.at[0], st_sem.at[0])]
+    own_o.append(fetch(wo.at[1], wot.at[1, worow(d)], own_sem.at[3]))
     own_s.append(fetch(state.at[1], st.at[1], st_sem.at[1]))
 
 
@@ -364,19 +365,23 @@
                 xg[1, slot(t, x, rows), :] = current
             send = gather_start(l)
             if l == 0:
-                for ll in range(2):
+                out_first(0)
+            if l == 0:
+                for ll in range(1):
                     for q in range(6):
                         remote(
                             weights[q].at[ll], wcat.at[ll, wrow(q)], wc_send.at[0], wc_recv.at[ll], t, sibling
                         ).start()
-                out_first(0)
             else:
                 out_second(1)
+        gather_relay(l, send)
         if l == 0:
             with scope("turn0"):
                 turn(0)
-        gather_relay(l, send)
-        if l == 0:
+            for q in range(6):
+                remote(
+                    weights[q].at[1], wcat.at[1, wrow(q)], wc_send.at[0], wc_recv.at[1], t, sibling
+                ).start()
             with scope("prepare0"):
                 for copy in small:
                     copy.wait()

time: 56.9 us -> 56.8 us (level)
  no operation moved by 1% of the time
where the time goes in v9:
time: 56.8 us; the launch traced here: 56.7 us
  Pallas kernels  56 us (99%)
  between operations  0.64 us (1%)
    pallas_call x1, Pallas kernels, step(): pl.pallas_call(functools.partial(step_body, tp=tp, dp=dp), out_shape=(plt...  52.7 us
    pallas_call x1, Pallas kernels, put(): pl.pallas_call(put_body, out_shape=(jax.ShapeDtypeStruct(mixed.shape, mix...  3.38 us

profile of v9, /device:TPU:0, one launch (start us, length us, event | category | flops | bytes accessed | tf_op | source)
XLA Modules:
  0.0 56.7 jit_solution(1816078724929830781)
XLA Ops:
  0.6 52.7 %step.1 = (bf16[32,256]{1,0:T(8,128)(2,1)S(1)}, f32[2,32,4,64,64]{4,3,2,1,0:T(8,128)S(1)}) custom-call(bf16[32,256]{1,0:T(8,128)(2,1)} %tok.1, s32[1,32]{1,0:T(1,128)} %bitcast.15, f32[2,4096]{1,0:T(2,128)} %gain_hbm.1, f32[2,256]{1,0:T(2,128)} %base_hbm.1, f32[2,256]{1,0:T(2,128)} %rate_hbm.1, f32[2,256]{1,0:T(2,128)} %ggain_hbm.1, ...), custom_call_target="tpu_custom_call" | custom-call | tf_op jit(solution)/shard_map/step/pallas_call | solution.py:424
  53.3 3.4 %put.1 = (bf16[32,256]{1,0:T(8,128)(2,1)}, f32[2,32,4,64,64]{4,3,2,1,0:T(8,128)}) custom-call(bf16[32,256]{1,0:T(8,128)(2,1)S(1)} %get-tuple-element.4.mixed_ref, f32[2,32,4,64,64]{4,3,2,1,0:T(8,128)S(1)} %get-tuple-element.5.state_ref), custom_call_target="tpu_custom_call" | custom-call | tf_op jit(solution)/shard_map/put/pallas_call | solution.py:488

commit v10 on v9

--- a/solution.py
+++ b/solution.py
@@ -190,7 +190,7 @@
             count = (nx - 1) * (rows - CUT[l]) + (0 if o == (0, 0) else nx * CUT[l])
             with scope(f"x{l}_{o[0]}_{o[1]}"):
                 arrived(xg.at[l, pl.ds(0, count)], fin_recv.at[tt])
-            if i == 3:
+            if i == 2:
                 after()
             block = xg[l, slot(tt, 0, nx * rows), :]
             cols = pl.ds(pl.multiple_of(tt * width, width), width)

time: 56.8 us -> 56.7 us (level)
  no operation moved by 1% of the time
where the time goes in v10:
time: 56.7 us; the launch traced here: 56.6 us
  Pallas kernels  56 us (99%)
  between operations  0.64 us (1%)
    pallas_call x1, Pallas kernels, step(): pl.pallas_call(functools.partial(step_body, tp=tp, dp=dp), out_shape=(plt...  52.6 us
    pallas_call x1, Pallas kernels, put(): pl.pallas_call(put_body, out_shape=(jax.ShapeDtypeStruct(mixed.shape, mix...  3.38 us

profile of v10, /device:TPU:0, one launch (start us, length us, event | category | flops | bytes accessed | tf_op | source)
XLA Modules:
  0.0 56.6 jit_solution(8752289300186840387)
XLA Ops:
  0.6 52.6 %step.1 = (bf16[32,256]{1,0:T(8,128)(2,1)S(1)}, f32[2,32,4,64,64]{4,3,2,1,0:T(8,128)S(1)}) custom-call(bf16[32,256]{1,0:T(8,128)(2,1)} %tok.1, s32[1,32]{1,0:T(1,128)} %bitcast.15, f32[2,4096]{1,0:T(2,128)} %gain_hbm.1, f32[2,256]{1,0:T(2,128)} %base_hbm.1, f32[2,256]{1,0:T(2,128)} %rate_hbm.1, f32[2,256]{1,0:T(2,128)} %ggain_hbm.1, ...), custom_call_target="tpu_custom_call" | custom-call | tf_op jit(solution)/shard_map/step/pallas_call | solution.py:424
  53.2 3.4 %put.1 = (bf16[32,256]{1,0:T(8,128)(2,1)}, f32[2,32,4,64,64]{4,3,2,1,0:T(8,128)}) custom-call(bf16[32,256]{1,0:T(8,128)(2,1)S(1)} %get-tuple-element.4.mixed_ref, f32[2,32,4,64,64]{4,3,2,1,0:T(8,128)S(1)} %get-tuple-element.5.state_ref), custom_call_target="tpu_custom_call" | custom-call | tf_op jit(solution)/shard_map/put/pallas_call | solution.py:488
